TPU v7x, 512 devices: a whole 4x4x16 slice. The times are simulated.
512 devices in a mesh: sp: 32 (over z, core), tp: 16 (over y, x).
Axes of the slice: x: 4, y: 4, z: 16, core: 2. Of those that a mesh axis runs over, the one named last changes fastest.
Arguments:
- residual: bfloat16 [6144, 2048], P('sp'), may hold values from -6 to 6
- query_in: bfloat16 [6144, 2048], P('sp', 'tp'), may hold values from -6 to 6
- value_in: bfloat16 [6144, 2048], P('sp', 'tp'), may hold values from -6 to 6
- forget_fwd: bfloat16 [6144, 2048], P('sp', 'tp'), may hold values from -4.5 to 4.5
- forget_bwd: bfloat16 [6144, 2048], P('sp', 'tp'), may hold values from -4.5 to 4.5
- jumps: float32 [16, 6144], P('tp', 'sp'), may hold values from -2.8 to 0
- gate_gap: float32 [2, 2048], P(None, 'tp'), may hold values from 0 to 0.1
- out_gate: bfloat16 [6144, 2048], P('sp', 'tp'), may hold values from -6 to 6
- head_gain: float32 [2048], P('tp'), may hold values from 0.1 to 1.9
- out_weight: bfloat16 [2048, 2048], P('tp'), may hold values from -0.25 to 0.25
- norm_gain: float32 [2048], replicated, may hold values from 0.1 to 1.9
- route_ids: int32 [6144, 4], P('sp'), may hold values from 0 to 31, all different within a row; in each aligned block of 192 rows (0 to 191, 192 to 383, ...) at most 36 rows name the same one
- route_weights: float32 [6144, 4], P('sp'), may hold values from 0.05 to 0.5
- w_gate: bfloat16 [32, 2048, 4096], P('sp', None, 'tp'), may hold values from -0.375 to 0.375
- w_up: bfloat16 [32, 2048, 4096], P('sp', None, 'tp'), may hold values from -0.375 to 0.375
- w_down: bfloat16 [32, 4096, 2048], P('sp', None, 'tp'), may hold values from -0.09375 to 0.09375
Outputs:
- mixed: bfloat16 [6144, 2048], P('sp', 'tp')
Inputs may be any that keep to these rules, and one draw needn't show every extreme that they name: `route_ids`: in each aligned block of 192 rows each expert is named by at most 36 rows, and by exactly 36 in some block; each row names 4 different experts.
All inputs are finite; a program needn't handle non-finite values.
Results may differ from a plain program's by a relative error of at most 0.024.
Values may be sent and summed in bfloat16 or wider, within the bound.
No kernel may reach another device: no remote copies, remote signals or barrier semaphores. Data moves between devices by JAX's collectives and lax.ppermute only.
A program may use at most 64 MiB of HBM per device.

v0:
```python
import math

import jax
import jax.numpy as jnp
from jax import lax
from jax.sharding import Mesh
from jax.sharding import PartitionSpec as P

EXPERTS = 32
CAP = 36
SP = ("sp_0", "sp_1")


highest_precision = lax.Precision.HIGHEST
eps_norm = 1e-06
limit_value = 7.0
alpha_value = 1.702


def filled_with(x, identity):
    return jax.tree.map(
        lambda a, e: jnp.broadcast_to(jnp.asarray(e, a.dtype), a.shape), x, identity
    )


def all_in_one(x, axis):
    leaves = jax.tree.leaves(x)
    turns = sorted(range(len(leaves)), key=lambda k: -leaves[k].size)
    width = (1, *leaves[turns[0]].shape)[-1]
    lines = [
        jnp.pad(leaves[k].reshape(-1), (0, -leaves[k].size % width)).reshape(-1, width)
        for k in turns
    ]
    both, at, found = (lax.all_gather(jnp.concatenate(lines), axis), 0, {})
    for k, line in zip(turns, lines):
        section = both[:, at : at + len(line)].reshape(len(both), -1)
        found[k] = section[:, : leaves[k].size].reshape(-1, *leaves[k].shape)
        at += len(line)
    numbers = iter(range(len(leaves)))
    return jax.tree.map(lambda _: found[next(numbers)], x)


def entering(x, axes, combine, identity, reverse):
    before = start = filled_with(x, identity)
    running = x
    for axis in reversed(axes):
        length, index = (lax.axis_size(axis), lax.axis_index(axis))
        pieces = all_in_one(
            jax.tree.map(
                lambda part, kind: part.astype(kind),
                running,
                jax.tree.map(lambda a: jnp.bfloat16 if a.dtype == jnp.float32 else a.dtype, x),
            ),
            axis,
        )
        inside, running = (start, start)
        for k in reversed(range(length)) if reverse else range(length):
            passed = k > index if reverse else k < index
            running = combine(
                running, jax.tree.map(lambda part, own: part[k].astype(own.dtype), pieces, x)
            )
            inside = jax.tree.map(lambda new, old: jnp.where(passed, new, old), running, inside)
        before = combine(inside, before)
    return before


def in_blocks(x, dim, length):
    shape = x.shape
    pieces = x.reshape(*shape[:dim], length, shape[dim] // length, *shape[dim + 1 :])
    return jnp.moveaxis(pieces, dim, 0)


def sent_and_summed(x, axis, dim):
    length = lax.axis_size(axis)
    pieces = lax.all_to_all(in_blocks(x, dim, length), axis, 0, 0, tiled=True)
    return jnp.sum(pieces.astype(jnp.float32), axis=0)


def rows_for(lines, length):
    spare = -lines.shape[0] % length
    if not spare:
        return lines
    return jnp.concatenate([lines, jnp.zeros((spare, *lines.shape[1:]), lines.dtype)])


def in_order(pieces, dim):
    pieces = jnp.moveaxis(pieces, 0, dim)
    shape = pieces.shape
    return pieces.reshape(*shape[:dim], shape[dim] * shape[dim + 1], *shape[dim + 2 :])


def sent_to_all(x, axis):
    copies = jnp.broadcast_to(x, (lax.axis_size(axis), *x.shape))
    return lax.all_to_all(copies, axis, split_axis=0, concat_axis=0, tiled=True)


def gather_directly(x, axis, dim):
    return in_order(sent_to_all(x, axis), dim)


def sum_by_parts(x, axes):
    lines = x.reshape(-1, x.shape[-1])
    own = sent_and_summed(rows_for(lines, lax.axis_size(axes)), axes, 0)
    whole = gather_directly(own.astype(jnp.bfloat16), axes, 0)
    return whole[: len(lines)].reshape(x.shape).astype(jnp.float32)


def turned_blocks(pieces, axes, turns):
    inside = pieces.shape[1:]
    filled = pieces.reshape(*(lax.axis_size(a) for a in axes), *inside)
    for k in turns:
        filled = lax.all_to_all(filled, axes[k], k, k, tiled=True)
    return filled.reshape(-1, *inside)


def core_and_chips(x, groups, turns, split_dim, concat_dim):
    length = lax.axis_size(groups[0]) * lax.axis_size(groups[1])
    pieces = in_blocks(x, split_dim, length)
    return in_order(turned_blocks(pieces, groups, turns), concat_dim)


def block_pass(queries, keys_in, values, logs):
    head_rows, head_count, head_width = queries.shape
    block_size = math.gcd(head_rows, 64)
    block_count = head_rows // block_size

    def to_blocks(array):
        return array.reshape(block_count, block_size, head_count, array.shape[-1])

    q_block, k_block, v_block, log_block = (
        to_blocks(queries),
        to_blocks(keys_in),
        to_blocks(values),
        to_blocks(logs),
    )
    decay_sums = jnp.cumsum(log_block, axis=1)
    middle = decay_sums[:, block_size // 2 - 1 : block_size // 2]
    scores = jnp.einsum(
        "nthk,nshk->nhts",
        q_block * jnp.exp(decay_sums - middle),
        k_block * jnp.exp(middle - decay_sums),
        precision=highest_precision,
    )
    lower_mask = jnp.tril(jnp.ones((block_size, block_size), bool))
    within = jnp.einsum(
        "nhts,nshv->nthv", jnp.where(lower_mask, scores, 0.0), v_block, precision=highest_precision
    )
    block_end = decay_sums[:, -1]
    q_start = q_block * jnp.exp(decay_sums)
    k_end = k_block * jnp.exp(block_end[:, None] - decay_sums)

    def advance(current_state, block_items):
        query_segment, key_segment, value_segment, decay_part = block_items
        state_readout = jnp.einsum(
            "qwe,wei->qwi", query_segment, current_state, precision=highest_precision
        )
        current_state = current_state * jnp.exp(decay_part)[:, :, None] + jnp.einsum(
            "foj,fox->ojx", key_segment, value_segment, precision=highest_precision
        )
        return (current_state, state_readout)

    zero_state = jnp.zeros((head_count, head_width, values.shape[-1]), jnp.float32)
    final_state, across = lax.scan(advance, zero_state, (q_start, k_end, v_block, block_end))
    return ((within + across).reshape(head_rows, head_count, -1), final_state)


def combine_states(first_part, second_part):
    return (
        first_part[0] * second_part[0],
        second_part[0][:, :, None] * first_part[1] + second_part[1],
    )


def carried(queries, logs, running_state):
    decayed_state = queries * jnp.exp(jnp.cumsum(logs, axis=0))
    return jnp.einsum("una,nae->une", decayed_state, running_state, precision=highest_precision)


def shards(
    residual,
    query_in,
    value_in,
    forget_fwd,
    forget_bwd,
    jumps,
    gate_gap,
    out_gate,
    head_gain,
    out_weight,
    norm_gain,
    route_ids,
    route_weights,
    w_gate,
    w_up,
    w_down,
):
    head_rows, local_width = query_in.shape
    head_count = jumps.shape[0]
    head_width = local_width // head_count

    def by_head(array):
        return array.astype(jnp.float32).reshape(head_rows, head_count, head_width)

    queries = jax.nn.silu(by_head(query_in))
    values = by_head(value_in)
    jump_rows = jnp.transpose(jumps)[:, :, None]

    def gate_terms(forget_in, gap):
        key_share = gap.reshape(head_count, head_width) * jax.nn.sigmoid(-by_head(forget_in))
        return (key_share, jnp.log1p(-key_share) + jump_rows)

    keys_fwd, logs_fwd = gate_terms(forget_fwd, gate_gap[0])
    keys_bwd, logs_bwd = gate_terms(forget_bwd, gate_gap[1])
    ones_part = jnp.ones((head_count, head_width), jnp.float32)
    zero_part = jnp.zeros((head_count, head_width, head_width), jnp.float32)
    local_fwd, final_fwd = block_pass(queries, keys_fwd, values, logs_fwd)
    summary_fwd = (jnp.exp(jnp.sum(logs_fwd, axis=0)), final_fwd)
    carry_fwd = entering(summary_fwd, SP, combine_states, (ones_part, zero_part), False)[1]
    flip_queries = jnp.flip(queries, 0)
    flip_logs = jnp.flip(logs_bwd, 0)
    local_bwd, final_bwd = block_pass(
        flip_queries, jnp.flip(keys_bwd, 0), jnp.flip(values, 0), flip_logs
    )
    summary_bwd = (jnp.exp(jnp.sum(logs_bwd, axis=0)), final_bwd)
    carry_bwd = entering(summary_bwd, SP, combine_states, (ones_part, zero_part), True)[1]
    forward_out = local_fwd + carried(queries, logs_fwd, carry_fwd)
    backward_out = jnp.flip(local_bwd + carried(flip_queries, flip_logs, carry_bwd), 0)
    mixed_heads = forward_out + backward_out
    mean_square = jnp.mean(mixed_heads * mixed_heads, axis=-1, keepdims=True)
    normed = (mixed_heads * lax.rsqrt(mean_square + eps_norm)).reshape(head_rows, local_width)
    gated = (normed * head_gain * jax.nn.silu(out_gate.astype(jnp.float32))).astype(jnp.bfloat16)
    head_terms = jnp.dot(gated, out_weight, preferred_element_type=jnp.float32)
    summed = sum_by_parts(head_terms.astype(jnp.bfloat16), "tp")
    stream = (residual.astype(jnp.float32) + summed).astype(jnp.bfloat16)
    stream_f = stream.astype(jnp.float32)
    row_scale = lax.rsqrt(jnp.mean(stream_f * stream_f, axis=-1, keepdims=True) + eps_norm)
    normed_rows = (stream_f * row_scale * norm_gain).astype(jnp.bfloat16)
    top_count = route_ids.shape[1]
    flat_ids = route_ids.reshape(-1)
    one_hot = (flat_ids[:, None] == jnp.arange(EXPERTS, dtype=jnp.int32)[None, :]).astype(jnp.int32)
    slot_rank = jnp.sum((jnp.cumsum(one_hot, axis=0) - 1) * one_hot, axis=1)
    slot_index = flat_ids * CAP + slot_rank
    owner_rows = jnp.arange(head_rows * top_count, dtype=jnp.int32) // top_count
    slot_rows = jnp.full((EXPERTS * CAP,), head_rows, jnp.int32).at[slot_index].set(owner_rows)
    padded_rows = jnp.concatenate(
        [normed_rows, jnp.zeros((1, normed_rows.shape[1]), jnp.bfloat16)], axis=0
    )
    tp_index = lax.axis_index("tp")
    part_width = w_down.shape[2]
    column_rows = lax.dynamic_slice_in_dim(padded_rows, tp_index * part_width, part_width, 1)
    buffer = column_rows[slot_rows].reshape(EXPERTS, CAP, part_width)
    arrived = lax.all_to_all(buffer, SP, split_axis=0, concat_axis=1, tiled=True)
    piece = lax.all_gather(arrived, "tp", axis=2, tiled=True)
    gate_sum = jnp.einsum("esd,edf->esf", piece, w_gate, preferred_element_type=jnp.float32)
    up_sum = jnp.einsum("esd,edf->esf", piece, w_up, preferred_element_type=jnp.float32)
    gate_sum = jnp.minimum(gate_sum, limit_value)
    up_sum = jnp.clip(up_sum, -limit_value, limit_value)
    active = (gate_sum * jax.nn.sigmoid(alpha_value * gate_sum) * (up_sum + 1.0)).astype(
        jnp.bfloat16
    )
    produced = jnp.einsum(
        "esf,efd->esd",
        lax.all_gather(active, "tp", axis=2, tiled=True),
        w_down,
        preferred_element_type=jnp.float32,
    ).astype(jnp.bfloat16)
    returned = core_and_chips(produced, ("sp_0", "sp_1"), (1, 0), 1, 0)
    picked = returned.reshape(EXPERTS * CAP, part_width)[slot_index].astype(jnp.float32)
    picked = picked.reshape(head_rows, top_count, part_width)
    moe_out = jnp.sum(picked * route_weights[:, :, None], axis=1)
    own_columns = lax.dynamic_slice_in_dim(stream_f, tp_index * part_width, part_width, 1)
    return (own_columns + moe_out).astype(jnp.bfloat16)


def solution(mesh):
    finer = Mesh(mesh.devices.reshape(16, 2, mesh.shape["tp"]), ("sp_0", "sp_1", "tp"))
    return jax.shard_map(
        shards,
        mesh=finer,
        in_specs=(
            P(SP, None),
            P(SP, "tp"),
            P(SP, "tp"),
            P(SP, "tp"),
            P(SP, "tp"),
            P("tp", SP),
            P(None, "tp"),
            P(SP, "tp"),
            P("tp"),
            P("tp", None),
            P(),
            P(SP, None),
            P(SP, None),
            P(SP, None, "tp"),
            P(SP, None, "tp"),
            P(SP, None, "tp"),
        ),
        out_specs=P(SP, "tp"),
        check_vma=False,
    )
```

profile of v0, /device:TPU:2, one launch (start us, length us, event | category | flops | bytes accessed | tf_op | source)
XLA Modules:
  0.0 397.6 jit_solution(2136767596949991621)
XLA Ops:
  6.5 0.8 slice_bitcast_fusion.35
  7.3 1.0 fusion.388
  8.4 0.8 convert_multiply_fusion.2
  9.2 0.8 convert_element_type.809
  10.1 0.5 copy_bitcast_fusion.2
  10.6 0.2 exponential_multiply_fusion.2
  10.9 1.7 while.26
  11.1 0.3 fusion.427
  11.7 0.3 fusion.427
  12.3 0.3 fusion.427
  12.6 1.9 all-gather.5
  14.5 0.6 broadcast_select_fusion.3
  15.2 38.4 %all-gather.6 = bf16[16,129,128]{2,1,0:T(8,128)(2,1)S(1)} all-gather(bf16[1,129,128]{2,1,0:T(8,128)(2,1)S(1)} %maximum_bitcast_fusion.1), channel_id=3, replica_groups=mesh['sp_0'=16,'sp_1'=2,'tp'=16] {'sp_0'}, dimensions={0}, use_global_device_ids=true | all-gather | bytes 561408 | tf_op jit(solution)/shard_map/all_gather | solution.py:34
  53.6 0.6 fusion.381
  54.2 0.5 fusion.366
  54.9 0.2 reverse.15
  55.2 0.2 reverse.13
  55.5 0.2 reverse.14
  55.7 0.6 copy_bitcast_fusion
  56.3 0.2 exponential_multiply_fusion
  56.6 1.7 while.27
  56.9 0.3 fusion.434
  57.4 0.3 fusion.434
  58.0 0.3 fusion.434
  58.4 1.9 all-gather.7
  60.2 0.6 broadcast_select_fusion.1
  61.0 29.2 %all-gather.8 = bf16[16,129,128]{2,1,0:T(8,128)(2,1)S(1)} all-gather(bf16[1,129,128]{2,1,0:T(8,128)(2,1)S(1)} %maximum_bitcast_fusion.3), channel_id=5, replica_groups=mesh['sp_0'=16,'sp_1'=2,'tp'=16] {'sp_0'}, dimensions={0}, use_global_device_ids=true | all-gather | bytes 561408 | tf_op jit(solution)/shard_map/all_gather | solution.py:34
  90.2 0.6 fusion.364
  90.8 0.5 fusion.349
  91.8 0.3 convolution_select_fusion
  92.2 1.1 fusion.41
  93.5 1.5 fusion.39
  95.0 0.2 rev.14
  95.3 0.3 convolution_select_fusion.1
  96.0 1.6 multiply_reduce_fusion.1
  97.7 0.4 convolution_convert_fusion
  98.1 1.2 reshape.1657
  99.3 7.5 %all-to-all-start = ((bf16[16,12,2048]{2,1,0:T(8,128)(2,1)}), bf16[16,12,2048]{2,1,0:T(8,128)(2,1)S(1)}, u32[]{:S(2)}, u32[]{:S(2)}) async-start(bf16[16,12,2048]{2,1,0:T(8,128)(2,1)} %reshape.1657), calls=%async_computation | async-start | bytes 2097152 | tf_op jit(solution)/shard_map/all_to_all | solution.py:75
  107.0 1.7 reduce-window.26
  108.7 9.9 %all-to-all-done = bf16[16,12,2048]{2,1,0:T(8,128)(2,1)S(1)} async-done(((bf16[16,12,2048]{2,1,0:T(8,128)(2,1)}), bf16[16,12,2048]{2,1,0:T(8,128)(2,1)S(1)}, u32[]{:S(2)}, u32[]{:S(2)}) %all-to-all-start) | async-done | bytes 786464 | tf_op jit(solution)/shard_map/all_to_all | solution.py:75
  118.8 1.1 broadcast_in_dim.35
  120.0 5.0 %all-to-all-start.1 = ((bf16[16,12,2048]{2,1,0:T(8,128)(2,1)}), bf16[16,12,2048]{2,1,0:T(8,128)(2,1)S(1)}, u32[]{:S(2)}, u32[]{:S(2)}) async-start(bf16[16,12,2048]{2,1,0:T(8,128)(2,1)} %broadcast_in_dim.35), calls=%async_computation.1 | async-start | bytes 2097152 | tf_op jit(solution)/shard_map/all_to_all | solution.py:94
  125.0 0.3 slice_reduce_fusion
  125.7 3.4 scatter_custom_fusion
  129.2 7.8 %all-to-all-done.1 = bf16[16,12,2048]{2,1,0:T(8,128)(2,1)S(1)} async-done(((bf16[16,12,2048]{2,1,0:T(8,128)(2,1)}), bf16[16,12,2048]{2,1,0:T(8,128)(2,1)S(1)}, u32[]{:S(2)}, u32[]{:S(2)}) %all-to-all-start.1) | async-done | bytes 786464 | tf_op jit(solution)/shard_map/all_to_all | solution.py:94
  136.9 1.3 reshape.1699
  138.3 1.7 multiply_reduce_fusion
  140.0 0.2 multiply_convert_fusion
  140.2 2.9 gather_fusion
  143.2 33.2 %all_to_all.32 = bf16[32,36,128]{2,1,0:T(8,128)(2,1)S(1)} all-to-all(bf16[32,36,128]{2,1,0:T(8,128)(2,1)S(1)} %reshape.1659), channel_id=1, replica_groups=mesh['sp_0'=16,'sp_1'=2,'tp'=16] {'sp_0','sp_1'}, dimensions={0} | all-to-all | bytes 589824 | tf_op jit(solution)/shard_map/all_to_all | solution.py:252
  176.5 0.8 all_to_all.24
  177.3 0.2 all-gather.14.cloned.1.call-start
  177.5 62.6 %all-gather.12.cloned.1.call-done = bf16[1,1152,2048]{2,1,0:T(8,128)(2,1)} async-done(((bf16[1,1152,128]{2,1,0:T(8,128)(2,1)}), bf16[1,1152,2048]{2,1,0:T(8,128)(2,1)}) %all-gather.12.cloned.1.call-update) | async-done | bytes 4718608 | tf_op jit(solution)/shard_map/all_gather | solution.py:253
  240.1 3.9 fusion.25
  244.1 2.4 fusion.34
  246.6 97.4 %all-gather.14.cloned.1.call-done = bf16[1152,4096]{1,0:T(8,128)(2,1)} async-done(((bf16[1152,256]{1,0:T(8,128)(2,1)}), bf16[1152,4096]{1,0:T(8,128)(2,1)}) %all-gather.14.cloned.1.call-update) | async-done | bytes 9437200 | tf_op jit(solution)/shard_map/all_gather | solution.py:263
  344.0 6.5 %convolution_convert_fusion.1 = bf16[1152,128]{1,0:T(8,128)(2,1)S(1)} fusion(bf16[1152,4096]{1,0:T(8,128)(2,1)} %all-gather.14.cloned.1.call-done, bf16[1,4096,128]{2,1,0:T(8,128)(2,1)} %param.35), kind=kOutput, calls=%fused_computation.43 | convolution fusion | flops 1208107008 | bytes 10780672 | tf_op jit(solution)/shard_map/esf,efd->esd/dot_general | solution.py:261
  350.7 4.0 all_to_all.33
  354.6 1.0 copy.64
  355.6 12.3 %all-to-all-start.4 = ((bf16[16,2,1,36,128]{4,1,3,2,0:T(2,128)(2,1)}), bf16[16,2,1,36,128]{4,1,3,2,0:T(2,128)(2,1)S(1)}, u32[]{:S(2)}, u32[]{:S(2)}) async-start(bf16[16,2,1,36,128]{4,1,3,2,0:T(2,128)(2,1)} %copy.64), calls=%async_computation.4 | async-start | bytes 589824 | tf_op jit(solution)/shard_map/all_to_all | solution.py:112
  368.1 19.8 %all-to-all-done.4 = bf16[16,2,1,36,128]{4,1,3,2,0:T(2,128)(2,1)S(1)} async-done(((bf16[16,2,1,36,128]{4,1,3,2,0:T(2,128)(2,1)}), bf16[16,2,1,36,128]{4,1,3,2,0:T(2,128)(2,1)S(1)}, u32[]{:S(2)}, u32[]{:S(2)}) %all-to-all-start.4) | async-done | bytes 294944 | tf_op jit(solution)/shard_map/all_to_all | solution.py:112
  387.9 1.9 gather_fusion.1
  389.8 0.3 fusion.46
  390.1 0.6 add_convert_fusion.1
  (172 shorter events, 4.4 us)
Async XLA Ops:
  6.5 233.5 %copy-start = (bf16[1,2048,256]{2,1,0:T(8,128)(2,1)S(1)}, bf16[1,2048,256]{2,1,0:T(8,128)(2,1)}, u32[]{:S(2)}) copy-start(bf16[1,2048,256]{2,1,0:T(8,128)(2,1)} %param.33) | copy-start | bytes 3145732
  10.9 44.1 %copy-start.3 = (bf16[192,128]{1,0:T(8,128)(2,1)S(1)}, bf16[192,128]{1,0:T(8,128)(2,1)}, u32[]{:S(2)}) copy-start(bf16[192,128]{1,0:T(8,128)(2,1)} %param.22) | copy-start | bytes 147460
  12.6 41.7 %copy-start.4 = (f32[3,64,1,128]{3,1,2,0:T(8,128)}, f32[3,64,1,128]{3,1,2,0:T(8,128)S(1)}, u32[]{:S(2)}) copy-start(f32[3,64,1,128]{3,1,2,0:T(8,128)S(1)} %get-tuple-element.81) | copy-start | bytes 294916
  14.5 40.9 %copy-start.7 = (bf16[2,129,128]{2,1,0:T(8,128)(2,1)}, bf16[2,129,128]{2,1,0:T(8,128)(2,1)S(1)}, u32[]{:S(2)}) copy-start(bf16[2,129,128]{2,1,0:T(8,128)(2,1)S(1)} %all-gather.5) | copy-start | bytes 198148
  14.5 40.9 %copy-start.19 = (f32[128]{0:T(128)}, f32[128]{0:T(128)S(1)}, u32[]{:S(2)}) copy-start(f32[128]{0:T(128)S(1)} %fusion.382) | copy-start | bytes 1540
  15.1 40.3 %copy-start.16 = (f32[128]{0:T(128)}, f32[128]{0:T(128)S(1)}, u32[]{:S(2)}) copy-start(f32[128]{0:T(128)S(1)} %get-tuple-element.212) | copy-start | bytes 1540
  58.3 2.6 copy-start.6
  58.3 33.5 %copy-start.12 = (f32[3,128]{1,0:T(4,128)S(1)}, f32[3,128]{1,0:T(4,128)}, u32[]{:S(2)}) copy-start(f32[3,128]{1,0:T(4,128)} %get-tuple-element.225) | copy-start | bytes 4612
  60.2 31.1 %copy-start.8 = (bf16[2,129,128]{2,1,0:T(8,128)(2,1)}, bf16[2,129,128]{2,1,0:T(8,128)(2,1)S(1)}, u32[]{:S(2)}) copy-start(bf16[2,129,128]{2,1,0:T(8,128)(2,1)S(1)} %all-gather.7) | copy-start | bytes 198148
  92.1 3.2 copy-start.11
  93.3 2.4 copy-start.5
  93.3 2.6 copy-start.10
  93.3 2.6 copy-start.17
  93.3 2.6 copy-start.20
  93.3 2.6 copy-start.21
  93.3 2.6 copy-start.22
  93.3 2.6 copy-start.23
  93.4 2.6 copy-start.24
  93.4 2.6 copy-start.25
  93.4 2.6 copy-start.26
  93.4 2.6 copy-start.27
  93.4 2.6 copy-start.28
  93.4 2.6 copy-start.29
  93.4 2.6 copy-start.30
  93.4 2.6 copy-start.31
  93.4 2.6 copy-start.32
  93.4 2.6 copy-start.33
  93.5 2.6 copy-start.34
  93.5 2.6 copy-start.35
  93.5 2.6 copy-start.36
  93.5 2.6 copy-start.39
  95.3 2.3 copy-start.2
  95.3 2.3 copy-start.9
  95.3 2.3 copy-start.18
  98.1 8.7 %copy-start.13 = (s32[192,4]{0,1:T(4,128)S(1)}, s32[192,4]{0,1:T(4,128)}, u32[]{:S(2)}) copy-start(s32[192,4]{0,1:T(4,128)} %param.31) | copy-start | bytes 9220
  99.3 19.4 %all-to-all-start = ((bf16[16,12,2048]{2,1,0:T(8,128)(2,1)}), bf16[16,12,2048]{2,1,0:T(8,128)(2,1)S(1)}, u32[]{:S(2)}, u32[]{:S(2)}) async-start(bf16[16,12,2048]{2,1,0:T(8,128)(2,1)} %reshape.1657), calls=%async_computation | async-start | bytes 2097152 | tf_op jit(solution)/shard_map/all_to_all | solution.py:75
  120.0 17.0 %all-to-all-start.1 = ((bf16[16,12,2048]{2,1,0:T(8,128)(2,1)}), bf16[16,12,2048]{2,1,0:T(8,128)(2,1)S(1)}, u32[]{:S(2)}, u32[]{:S(2)}) async-start(bf16[16,12,2048]{2,1,0:T(8,128)(2,1)} %broadcast_in_dim.35), calls=%async_computation.1 | async-start | bytes 2097152 | tf_op jit(solution)/shard_map/all_to_all | solution.py:94
  124.9 115.1 %all-gather.12.cloned.1.call-start = ((), (), s32[]{:S(2)}) async-start(), calls=%async_computation.5 | async-start | bytes 5013504 | tf_op jit(solution)/shard_map/all_gather | solution.py:253
  125.2 13.1 %copy-start.1 = (bf16[192,2048]{1,0:T(8,128)(2,1)S(1)}, bf16[192,2048]{1,0:T(8,128)(2,1)}, u32[]{:S(2)}) copy-start(bf16[192,2048]{1,0:T(8,128)(2,1)} %param.20) | copy-start | bytes 2359300
  138.3 1.7 copy-start.14
  177.3 166.7 %all-gather.14.cloned.1.call-start = ((), (), s32[]{:S(2)}) async-start(), calls=%async_computation.6 | async-start | bytes 10027008 | tf_op jit(solution)/shard_map/all_gather | solution.py:263
  240.1 3.9 copy-start.37
  240.1 4.1 %copy-start.38 = (bf16[1,2048,256]{2,1,0:T(8,128)(2,1)S(1)}, bf16[1,2048,256]{2,1,0:T(8,128)(2,1)}, u32[]{:S(2)}) copy-start(bf16[1,2048,256]{2,1,0:T(8,128)(2,1)} %param.34) | copy-start | bytes 3145732
  350.5 17.4 %copy-start.15 = (f32[192,4]{0,1:T(4,128)S(1)}, f32[192,4]{0,1:T(4,128)}, u32[]{:S(2)}) copy-start(f32[192,4]{0,1:T(4,128)} %param.32) | copy-start | bytes 9220
  355.6 32.2 %all-to-all-start.4 = ((bf16[16,2,1,36,128]{4,1,3,2,0:T(2,128)(2,1)}), bf16[16,2,1,36,128]{4,1,3,2,0:T(2,128)(2,1)S(1)}, u32[]{:S(2)}, u32[]{:S(2)}) async-start(bf16[16,2,1,36,128]{4,1,3,2,0:T(2,128)(2,1)} %copy.64), calls=%async_computation.4 | async-start | bytes 589824 | tf_op jit(solution)/shard_map/all_to_all | solution.py:112
Sparse Core Ops, SparseCore 0:
  177.4 62.6 all-gather.11
  246.7 97.2 all-gather.13
where the time goes:
time: 398 us
  waiting for transfers between devices  197 us (49%)
  blocking collectives  108 us (27%)
  starting transfers between devices  25 us (6%)
  matrix products  21.1 us (5%)
  local copies, waits for them, and re-layouts  18.4 us (5%)
  between operations  14.5 us (4%)
  other arithmetic  12.4 us (3%)
    all_gather x1, waiting for transfers between devices, shards(): lax.all_gather(active, 'tp', axis=2, tiled=True)  97.4 us
    all_gather x4, blocking collectives, all_in_one(): both, at, found = (lax.all_gather(jnp.concatenate(lines), axis), 0, {})  71.3 us
    all_gather x1, waiting for transfers between devices, shards(): piece = lax.all_gather(arrived, 'tp', axis=2, tiled=True)  62.6 us
    all_to_all x1, blocking collectives, shards(): lax.all_to_all(buffer, SP, split_axis=0, concat_axis=1, tiled=True)  33.2 us
    all_to_all x1, waiting for transfers between devices, turned_blocks(): filled = lax.all_to_all(filled, axes[k], k, k, tiled=True)  19.8 us
    all_to_all x1, starting transfers between devices, turned_blocks(): filled = lax.all_to_all(filled, axes[k], k, k, tiled=True)  12.3 us
    all_to_all x1, waiting for transfers between devices, sent_and_summed(): pieces = lax.all_to_all(in_blocks(x, dim, length), axis, 0, 0, tiled=True)  9.91 us
  transfers between devices with their start and end apart: 5, of which 5 were waited for; matrix products, arithmetic and copies ran while one was open for 2% of the time, Pallas kernels for 0%

commit v1 on v0

v1 whole, which is shorter than its diff:
```python
import jax
import jax.numpy as jnp
from jax import lax
from jax.experimental import pallas as pl
from jax.experimental.pallas import tpu as pltpu
from jax.sharding import Mesh
from jax.sharding import PartitionSpec as P

F32 = jnp.float32
BF16 = jnp.bfloat16
HI = lax.Precision.HIGHEST
EPS = 1e-06
CAP = 36
PAIR = 2 * CAP
Z = 16
R = 192
W = 128
D = 2048
SLOTS = 1152
SIDE = 4
TP = SIDE * SIDE
HID = 256
SP = ("z", "c")
PLANE = ("y", "x")
CYX = ("c", "y", "x")


def place(c, y, x):
    return (c * SIDE + y) * SIDE + x


FOUR = range(SIDE)
FIRST = [[place(0, y, x) for x in FOUR] for y in FOUR] + [
    [place(1, y, x) for y in FOUR] for x in FOUR
]
SECOND = [[place(0, y, x) for y in FOUR] for x in FOUR] + [
    [place(1, y, x) for x in FOUR] for y in FOUR
]


def exchange(pieces, groups):
    return lax.all_to_all(pieces, CYX, 0, 0, axis_index_groups=groups, tiled=True)


def spread(x, groups):
    return exchange(jnp.broadcast_to(x, (SIDE, *x.shape)), groups)


def dot(a, b, dims, precision=None):
    return lax.dot_general(a, b, (dims, ((), ())), precision=precision, preferred_element_type=F32)


def iota2(shape, dim):
    return lax.broadcasted_iota(jnp.int32, shape, dim)


def head_body(q_ref, v_ref, ff_ref, fb_ref, jr_ref, jc_ref, gap_ref, local_ref, qs_ref, sum_ref):
    q = q_ref[...].astype(F32)
    q = q * jax.nn.sigmoid(q)
    v = v_ref[...].astype(F32)
    row = iota2((R, R), 0)
    col = iota2((R, R), 1)
    jr = jr_ref[...]
    jc = jc_ref[...]
    total = None
    for d, f_ref in enumerate((ff_ref, fb_ref)):
        seen = (col <= row) if d == 0 else (col >= row)
        seen_t = (row <= col) if d == 0 else (row >= col)
        key = gap_ref[d : d + 1, :] * jax.nn.sigmoid(-f_ref[...].astype(F32))
        sums = dot(seen.astype(F32), jnp.log1p(-key), ((1,), (0,)), HI)
        jump_c = jnp.sum(jnp.where(seen, jr, 0.0), axis=1, keepdims=True)
        jump_r = jnp.sum(jnp.where(seen_t, jc, 0.0), axis=0, keepdims=True)
        mid = sums[R // 2 : R // 2 + 1, :]
        scores = dot(q * jnp.exp(sums - mid), key * jnp.exp(mid - sums), ((1,), (1,)), HI)
        fade = jnp.exp(jnp.where(seen, jump_c - jump_r, -1e30))
        part = dot(scores * fade, v, ((1,), (0,)), HI)
        total = part if total is None else total + part
        last = R - 1 if d == 0 else 0
        end = sums[last : last + 1, :]
        end_jump = jump_c[last : last + 1, :]
        key_end = key * jnp.exp((end - sums) + (end_jump - jump_c))
        sum_ref[d, 0:W, :] = dot(v, key_end, ((0,), (0,)), HI)
        sum_ref[d, W : W + 8, :] = jnp.broadcast_to(jnp.exp(end + end_jump), (8, W))
        qs_ref[d] = q * jnp.exp(sums + jump_c)
    local_ref[...] = total


def pack_body(at_ref, sum_ref, out_ref):
    z = at_ref[0]
    c = at_ref[1]
    start = pl.multiple_of(c * (W // 2), W // 2)

    def message(d):
        near, far = (1, 0) if d == 0 else (0, 1)
        near_decay = sum_ref[near, d, W : W + 1, :]
        decay = sum_ref[far, d, W : W + 1, :] * near_decay
        state = (
            sum_ref[far, d, pl.ds(start, W // 2), :] * near_decay
            + sum_ref[near, d, pl.ds(start, W // 2), :]
        )
        high = decay.astype(BF16).astype(F32)
        low = decay - high
        line = iota2((8, W), 0)
        tail = jnp.where(line == 0, high, jnp.where(line == 1, low, 0.0))
        return jnp.concatenate([state, tail], axis=0).astype(BF16)

    fwd = message(0)
    bwd = message(1)
    for k in range(Z):
        later = jnp.full((W // 2 + 8, W), k, jnp.int32) > z
        out_ref[k] = jnp.where(later, fwd.astype(F32), bwd.astype(F32)).astype(BF16)


def carry_body(at_ref, got_ref, out_ref):
    z = at_ref[0]

    def step(k, carry):
        got = got_ref[k].astype(F32)
        return carry * (got[W // 2 : W // 2 + 1] + got[W // 2 + 1 : W // 2 + 2]) + got[: W // 2]

    zero = jnp.zeros((W // 2, W), F32)
    out_ref[0] = lax.fori_loop(0, z, step, zero)
    out_ref[1] = lax.fori_loop(0, Z - 1 - z, lambda k, s: step(Z - 1 - k, s), zero)


def mix_body(at_ref, local_ref, qs_ref, sum_ref, carry_ref, gate_ref, gain_ref, w_ref, out_ref):
    c = at_ref[1]
    o = local_ref[...]
    for d in range(2):
        carry = jnp.concatenate([carry_ref[0, d], carry_ref[1, d]], axis=0)
        through = carry * sum_ref[d, d, W : W + 1, :] + sum_ref[d, d, 0:W, :]
        passed = jnp.full((W, W), c, jnp.int32) != d
        o = o + dot(qs_ref[d], jnp.where(passed, through, carry), ((1,), (1,)), HI)
    mean_square = jnp.mean(o * o, axis=1, keepdims=True)
    gate = gate_ref[...].astype(F32)
    gated = o * lax.rsqrt(mean_square + EPS) * gain_ref[...] * (gate * jax.nn.sigmoid(gate))
    terms = dot(gated.astype(BF16), w_ref[...], ((1,), (0,))).astype(BF16)
    for k in range(TP):
        out_ref[k] = terms[:, k * W : (k + 1) * W]


def slots_of(ids):
    expert = iota2((32, R), 0)
    named = ids[0:1] == expert
    for j in range(1, 4):
        named = named | (ids[j : j + 1] == expert)
    before = (iota2((R, R), 0) < iota2((R, R), 1)).astype(BF16)
    rank = dot(named.astype(BF16), before, ((1,), (0,)))
    return jnp.where(named, rank, -1000.0)


def send_body(at_ref, got_ref, res_ref, ids_ref, stream_ref, out_ref):
    total = got_ref[0].astype(F32)
    for k in range(1, TP):
        total = total + got_ref[k].astype(F32)
    stream = (res_ref[...].astype(F32) + total).astype(BF16)
    stream_ref[...] = stream
    slots = slots_of(ids_ref[...])
    line = iota2((PAIR, R), 0).astype(F32)
    for z in range(Z):
        hit = (line == slots[2 * z : 2 * z + 1]) | (line == slots[2 * z + 1 : 2 * z + 2] + CAP)
        out_ref[z] = dot(hit.astype(BF16), stream, ((1,), (0,))).astype(BF16)


def up_body(perm_ref, x_ref, gain_ref, wg_ref, wu_ref, out_ref, rows_ref):
    squares = None
    for j in range(TP):
        x = x_ref[perm_ref[j]].astype(F32)
        part = x * x
        squares = part if squares is None else squares + part
    scale = lax.rsqrt(jnp.sum(squares, axis=1, keepdims=True) / D + EPS)
    for j in range(TP):
        x = x_ref[perm_ref[j]].astype(F32)
        cols = pl.ds(j * W, W)
        rows_ref[:, cols] = (x * scale * gain_ref[:, cols]).astype(BF16)
    rows = rows_ref[...]
    c = jnp.minimum(dot(rows, wg_ref[...], ((1,), (0,))), 7.0)
    u = jnp.clip(dot(rows, wu_ref[...], ((1,), (0,))), -7.0, 7.0)
    active = (c * jax.nn.sigmoid(1.702 * c) * (u + 1.0)).astype(BF16)
    for k in range(SIDE):
        out_ref[k] = active


def down_body(act_ref, w_ref, out_ref, whole_ref):
    @pl.when(pl.program_id(0) == 0)
    def _():
        for k in range(SIDE):
            whole_ref[:, k * W : (k + 1) * W] = w_ref[k]

    active = jnp.concatenate([act_ref[k] for k in range(SIDE)], axis=1)
    made = dot(active, whole_ref[...], ((1,), (0,))).astype(BF16)
    for k in range(SIDE):
        out_ref[k] = made[:, k * W : (k + 1) * W]


def return_body(got_ref, stream_ref, ids_ref, weights_ref, out_ref):
    ids = ids_ref[...]
    weights = weights_ref[...]
    slots = slots_of(ids)
    expert = iota2((32, R), 0)
    share = jnp.where(ids[0:1] == expert, weights[0:1], 0.0)
    for j in range(1, 4):
        share = share + jnp.where(ids[j : j + 1] == expert, weights[j : j + 1], 0.0)
    line = iota2((PAIR, R), 0).astype(F32)
    total = jnp.zeros((R, W), F32)
    for z in range(Z):
        a = slice(2 * z, 2 * z + 1)
        b = slice(2 * z + 1, 2 * z + 2)
        share_at = jnp.where(line == slots[a], share[a], 0.0)
        share_at = share_at + jnp.where(line == slots[b] + CAP, share[b], 0.0)
        high = share_at.astype(BF16)
        low = (share_at - high.astype(F32)).astype(BF16)
        got = got_ref[z]
        total = total + (dot(high, got, ((0,), (0,))) + dot(low, got, ((0,), (0,))))
    out_ref[...] = (stream_ref[...].astype(F32) + total).astype(BF16)


VMEM = pl.BlockSpec(memory_space=pltpu.VMEM)
SMEM = pl.BlockSpec(memory_space=pltpu.SMEM)


def whole(body, outs, specs, name):
    return pl.pallas_call(
        body,
        out_shape=[jax.ShapeDtypeStruct(s, t) for s, t in outs],
        in_specs=specs,
        out_specs=[VMEM] * len(outs),
        name=name,
    )


def shards(
    residual,
    query_in,
    value_in,
    forget_fwd,
    forget_bwd,
    jumps,
    gate_gap,
    out_gate,
    head_gain,
    out_weight,
    norm_gain,
    route_ids,
    route_weights,
    w_gate,
    w_up,
    w_down,
):
    z = lax.axis_index("z")
    c = lax.axis_index("c")
    tp = lax.axis_index(PLANE)
    at = jnp.stack([z, c]).astype(jnp.int32)
    ids = route_ids.T
    weights = route_weights.T

    down = w_down.reshape(SIDE, SIDE, HID, W)
    down = jnp.where(c == 0, down, down.transpose(1, 0, 2, 3)).reshape(SIDE, SIDE * HID, W)
    down = exchange(down, SECOND)

    local, qs, summary = whole(
        head_body,
        (((R, W), F32), ((2, R, W), F32), ((2, W + 8, W), F32)),
        [VMEM] * 7,
        "head",
    )(query_in, value_in, forget_fwd, forget_bwd, jumps, jumps.reshape(R, 1), gate_gap)
    both = lax.all_gather(summary, "c")
    (packed,) = whole(pack_body, (((Z, W // 2 + 8, W), BF16),), [SMEM, VMEM], "pack")(at, both)
    packed = lax.all_to_all(packed, "z", 0, 0, tiled=True)
    (half,) = whole(carry_body, (((2, W // 2, W), F32),), [SMEM, VMEM], "carry")(at, packed)
    carry = lax.all_gather(half, "c")
    (terms,) = whole(mix_body, (((TP, R, W), BF16),), [SMEM] + [VMEM] * 7, "mix")(
        at, local, qs, both, carry, out_gate, head_gain.reshape(1, W), out_weight
    )
    terms = lax.all_to_all(terms, PLANE, 0, 0, tiled=True)

    own_residual = lax.dynamic_slice_in_dim(residual, tp * W, W, 1)
    stream, buffer = whole(
        send_body,
        (((R, W), BF16), ((Z, PAIR, W), BF16)),
        [SMEM] + [VMEM] * 3,
        "send",
    )(at, terms, own_residual, ids)

    arrived = lax.all_to_all(buffer, "z", 0, 0, tiled=True)
    arrived = arrived.reshape(Z, 2, CAP, W).transpose(1, 0, 2, 3).reshape(2, Z * CAP, W)
    rows = lax.all_to_all(arrived, "c", 0, 0, tiled=True).reshape(SLOTS, W)
    rows = spread(spread(rows, FIRST), SECOND).reshape(TP, SLOTS, W)

    j = jnp.arange(TP, dtype=jnp.int32)
    perm = jnp.where(c == 0, j, (j % SIDE) * SIDE + j // SIDE)
    step = 192
    active = pl.pallas_call(
        up_body,
        grid_spec=pltpu.PrefetchScalarGridSpec(
            num_scalar_prefetch=1,
            grid=(SLOTS // step,),
            in_specs=[
                pl.BlockSpec((TP, step, W), lambda i, p: (0, i, 0)),
                pl.BlockSpec((1, D), lambda i, p: (0, 0)),
                pl.BlockSpec((D, HID), lambda i, p: (0, 0)),
                pl.BlockSpec((D, HID), lambda i, p: (0, 0)),
            ],
            out_specs=pl.BlockSpec((SIDE, step, HID), lambda i, p: (0, i, 0)),
            scratch_shapes=[pltpu.VMEM((step, D), BF16)],
        ),
        out_shape=jax.ShapeDtypeStruct((SIDE, SLOTS, HID), BF16),
        name="up",
    )(perm, rows, norm_gain.reshape(1, D), w_gate[0], w_up[0])

    active = exchange(active, FIRST)
    made = pl.pallas_call(
        down_body,
        grid=(SLOTS // step,),
        in_specs=[
            pl.BlockSpec((SIDE, step, HID), lambda i: (0, i, 0)),
            pl.BlockSpec((SIDE, SIDE * HID, W), lambda i: (0, 0, 0)),
        ],
        out_specs=pl.BlockSpec((SIDE, step, W), lambda i: (0, i, 0)),
        out_shape=jax.ShapeDtypeStruct((SIDE, SLOTS, W), BF16),
        scratch_shapes=[pltpu.VMEM((SIDE * HID, SIDE * W), BF16)],
        name="down",
    )(active, down)
    made = exchange(made, SECOND)
    produced = jnp.sum(made.astype(F32), axis=0).astype(BF16)

    back = lax.all_to_all(produced.reshape(2, Z * CAP, W), "c", 0, 0, tiled=True)
    back = back.reshape(2, Z, CAP, W).transpose(1, 0, 2, 3).reshape(Z, PAIR, W)
    back = lax.all_to_all(back, "z", 0, 0, tiled=True)
    (mixed,) = whole(return_body, (((R, W), BF16),), [VMEM] * 4, "back")(
        back, stream, ids, weights
    )
    return mixed


def solution(mesh):
    finer = Mesh(mesh.devices.reshape(Z, 2, SIDE, SIDE), ("z", "c", "y", "x"))
    return jax.shard_map(
        shards,
        mesh=finer,
        in_specs=(
            P(SP, None),
            P(SP, PLANE),
            P(SP, PLANE),
            P(SP, PLANE),
            P(SP, PLANE),
            P(PLANE, SP),
            P(None, PLANE),
            P(SP, PLANE),
            P(PLANE),
            P(PLANE, None),
            P(),
            P(SP, None),
            P(SP, None),
            P(SP, None, PLANE),
            P(SP, None, PLANE),
            P(SP, None, PLANE),
        ),
        out_specs=P(SP, PLANE),
        check_vma=False,
    )
```

time: 398 us -> 255 us (0.64)
  waiting for transfers between devices: 197 us -> 43.7 us
  blocking collectives: 108 us -> 153 us
  Pallas kernels: 0 us -> 30.9 us
  matrix products: 21.1 us -> 0 us
  between operations: 14.5 us -> 0.09 us
  local copies, waits for them, and re-layouts: 18.4 us -> 7.09 us
  other arithmetic: 12.4 us -> 2.45 us
  starting transfers between devices: 25 us -> 16.1 us
    all_gather x2 -> x0, waiting for transfers between devices: 160 us -> none  [the longest x1 97.4 us: shards(): lax.all_gather(active, 'tp', axis=2, tiled=True)]
    all_to_all x2 -> x8, blocking collectives: 37.2 us -> 146 us  [the longest x3 51.7 us: exchange(): lax.all_to_all(pieces, CYX, 0, 0, axis_index_groups=groups, tiled=True)]
    all_gather x4 -> x2, blocking collectives: 71.3 us -> 7.47 us  [the longest x1 4.12 us: shards(): both = lax.all_gather(summary, 'c')]
    pallas_call x0 -> x8, Pallas kernels: none -> 30.9 us  [the longest x1 9.1 us: shards(): pl.pallas_call(up_body, grid_spec=pltpu.PrefetchScalarGridSpec(num_scalar...]
    dot_general x22 -> x0, matrix products: 21.1 us -> none  [the longest x1 6.53 us: shards(): jnp.einsum('esf,efd->esd', lax.all_gather(active, 'tp', axis=2, tiled=Tru...]
    all_to_all x3, starting transfers between devices: 24.7 us -> 16.1 us  [the longest x2 8.59 us: exchange(): lax.all_to_all(pieces, CYX, 0, 0, axis_index_groups=groups, tiled=True)]
    all_to_all x3, waiting for transfers between devices: 37.4 us -> 43.7 us  [the longest x2 30.8 us: exchange(): lax.all_to_all(pieces, CYX, 0, 0, axis_index_groups=groups, tiled=True)]
    gather x2 -> x0, local copies, waits for them, and re-layouts: 4.81 us -> none  [the longest x1 2.93 us: shards(): buffer = column_rows[slot_rows].reshape(EXPERTS, CAP, part_width)]
  transfers between devices with their start and end apart: 5 -> 3, of which waited for: 5 -> 3; matrix products, arithmetic and copies ran while one was open for 2% -> 1% of each run, Pallas kernels for 0% -> 4%
where the time goes in v1:
time: 255 us; the launch traced here: 254 us
  blocking collectives  153 us (60%)
  waiting for transfers between devices  43.7 us (17%)
  Pallas kernels  30.9 us (12%)
  starting transfers between devices  16.1 us (6%)
  local copies, waits for them, and re-layouts  7.09 us (3%)
    all_to_all x3, blocking collectives, exchange(): lax.all_to_all(pieces, CYX, 0, 0, axis_index_groups=groups, tiled=True)  51.7 us
    all_to_all x1, blocking collectives, shards(): packed = lax.all_to_all(packed, 'z', 0, 0, tiled=True)  35.4 us
    all_to_all x2, waiting for transfers between devices, exchange(): lax.all_to_all(pieces, CYX, 0, 0, axis_index_groups=groups, tiled=True)  30.8 us
    all_to_all x1, blocking collectives, shards(): back = lax.all_to_all(back, 'z', 0, 0, tiled=True)  25.8 us
    all_to_all x1, blocking collectives, shards(): arrived = lax.all_to_all(buffer, 'z', 0, 0, tiled=True)  25 us
    all_to_all x1, waiting for transfers between devices, shards(): terms = lax.all_to_all(terms, PLANE, 0, 0, tiled=True)  12.9 us
    pallas_call x1, Pallas kernels, shards(): pl.pallas_call(up_body, grid_spec=pltpu.PrefetchScalarGridSpec(num_scalar...  9.1 us
    all_to_all x2, starting transfers between devices, exchange(): lax.all_to_all(pieces, CYX, 0, 0, axis_index_groups=groups, tiled=True)  8.59 us
  transfers between devices with their start and end apart: 3, of which 3 were waited for; matrix products, arithmetic and copies ran while one was open for 1% of the time, Pallas kernels for 4%

profile of v1, /device:TPU:2, one launch (start us, length us, event | category | flops | bytes accessed | tf_op | source)
XLA Modules:
  0.0 253.5 jit_solution(8763324510688568963)
XLA Ops:
  0.0 0.0 copy-start
  0.0 1.5 copy.32.jc_ref
  1.5 3.9 %head.1 = (f32[192,128]{1,0:T(8,128)}, f32[2,192,128]{2,1,0:T(8,128)}, f32[2,136,128]{2,1,0:T(8,128)}) custom-call(bf16[192,128]{1,0:T(8,128)(2,1)} %q_ref.1, bf16[192,128]{1,0:T(8,128)(2,1)} %v_ref.1, bf16[192,128]{1,0:T(8,128)(2,1)} %ff_ref.1, bf16[192,128]{1,0:T(8,128)(2,1)} %fb_ref.1, f32[1,192]{1,0:T(1,128)} %jr_ref.1, f32[192,1]{1,0:T(8,128)} %copy.32.jc_ref, ...), custom_call_target="tpu_custom_call" | custom-call | tf_op jit(solution)/shard_map/head/pallas_call | solution.py:261
  5.4 4.1 %all-gather = f32[4,136,128]{2,1,0:T(8,128)} all-gather(f32[2,136,128]{2,1,0:T(8,128)} %get-tuple-element.12), channel_id=2, replica_groups=mesh['z'=16,'c'=2,'y'=4,'x'=4] {'c'}, dimensions={0}, use_global_device_ids=true | all-gather | bytes 417792 | tf_op jit(solution)/shard_map/all_gather | solution.py:267
  9.6 0.6 pad_add_fusion.at_ref
  10.1 1.7 pack.1
  11.9 35.4 %all_to_all.55.got_ref = bf16[16,72,128]{2,1,0:T(8,128)(2,1)} all-to-all(bf16[16,72,128]{2,1,0:T(8,128)(2,1)} %pack.1), channel_id=1, replica_groups=mesh['z'=16,'c'=2,'y'=4,'x'=4] {'z'}, dimensions={0} | all-to-all | bytes 589824 | tf_op jit(solution)/shard_map/all_to_all | solution.py:269
  47.2 1.7 carry.1
  49.0 3.3 %all-gather.1 = f32[4,64,128]{2,1,0:T(8,128)} all-gather(f32[2,64,128]{2,1,0:T(8,128)} %carry.1), channel_id=3, replica_groups=mesh['z'=16,'c'=2,'y'=4,'x'=4] {'c'}, dimensions={0}, use_global_device_ids=true | all-gather | bytes 196608 | tf_op jit(solution)/shard_map/all_gather | solution.py:271
  52.3 3.4 %mix.1 = bf16[16,192,128]{2,1,0:T(8,128)(2,1)} custom-call(s32[2]{0:T(128)} %pad_add_fusion.at_ref, f32[192,128]{1,0:T(8,128)} %get-tuple-element.10.local_ref, f32[2,192,128]{2,1,0:T(8,128)} %get-tuple-element.11.qs_ref, f32[2,2,136,128]{3,2,1,0:T(8,128)} %bitcast.27, f32[2,2,64,128]{3,2,1,0:T(8,128)} %bitcast.37, bf16[192,128]{1,0:T(8,128)(2,1)} %gate_ref.1, ...), custom_call_target="tpu_custom_call" | custom-call | tf_op jit(solution)/shard_map/mix/pallas_call | solution.py:272
  55.7 7.5 %all-to-all-start.1 = ((bf16[16,192,128]{2,1,0:T(8,128)(2,1)}), bf16[16,192,128]{2,1,0:T(8,128)(2,1)S(1)}, u32[]{:S(2)}, u32[]{:S(2)}) async-start(bf16[16,192,128]{2,1,0:T(8,128)(2,1)} %mix.1), calls=%async_computation.1 | async-start | bytes 1572864 | tf_op jit(solution)/shard_map/all_to_all | solution.py:275
  63.2 0.0 copy-done
  63.2 0.6 constant_dynamic-slice_fusion.res_ref
  63.8 12.9 %all-to-all-done.1.got_ref = bf16[16,192,128]{2,1,0:T(8,128)(2,1)S(1)} async-done(((bf16[16,192,128]{2,1,0:T(8,128)(2,1)}), bf16[16,192,128]{2,1,0:T(8,128)(2,1)S(1)}, u32[]{:S(2)}, u32[]{:S(2)}) %all-to-all-start.1) | async-done | bytes 786464 | tf_op jit(solution)/shard_map/all_to_all | solution.py:275
  76.7 0.0 copy-start.2
  76.7 0.9 copy-done.2
  77.6 2.4 send.1
  80.0 25.0 %all_to_all.56 = bf16[16,72,128]{2,1,0:T(8,128)(2,1)S(1)} all-to-all(bf16[16,72,128]{2,1,0:T(8,128)(2,1)} %get-tuple-element.13), channel_id=1, replica_groups=mesh['z'=16,'c'=2,'y'=4,'x'=4] {'z'}, dimensions={0} | all-to-all | bytes 589824 | tf_op jit(solution)/shard_map/all_to_all | solution.py:285
  105.1 0.3 copy.34
  105.4 4.0 %all_to_all.57 = bf16[2,576,128]{2,1,0:T(8,128)(2,1)S(1)} all-to-all(bf16[2,576,128]{2,1,0:T(8,128)(2,1)S(1)} %copy.35), channel_id=1, replica_groups=mesh['z'=16,'c'=2,'y'=4,'x'=4] {'c'}, dimensions={0} | all-to-all | bytes 589824 | tf_op jit(solution)/shard_map/all_to_all | solution.py:287
  109.4 0.2 broadcast_in_dim.6
  109.6 14.2 %all_to_all.58 = bf16[4,1152,128]{2,1,0:T(8,128)(2,1)S(1)} all-to-all(bf16[4,1152,128]{2,1,0:T(8,128)(2,1)S(1)} %broadcast_in_dim.6), channel_id=1, replica_groups={{0,1,2,3},{4,5,6,7},{8,9,10,11},{12,13,14,15},{16,20,24,28},{17,21,25,2..., dimensions={0} | all-to-all | bytes 2359296 | tf_op jit(solution)/shard_map/all_to_all | solution.py:42
  123.8 3.1 %broadcast_in_dim.7 = bf16[4,4,1152,128]{3,2,1,0:T(8,128)(2,1)} broadcast(bf16[4,1152,128]{2,1,0:T(8,128)(2,1)S(1)} %all_to_all.58), dimensions={1,2,3} | broadcast | bytes 5898240 | tf_op jit(solution)/shard_map/broadcast_in_dim | solution.py:46
  126.9 0.0 copy-start.3
  126.9 5.1 %all-to-all-start.5 = ((bf16[4,4,1152,128]{3,2,1,0:T(8,128)(2,1)}), bf16[4,4,1152,128]{3,2,1,0:T(8,128)(2,1)}, u32[]{:S(2)}, u32[]{:S(2)}) async-start(bf16[4,4,1152,128]{3,2,1,0:T(8,128)(2,1)} %broadcast_in_dim.7), calls=%async_computation.5 | async-start | bytes 9437184 | tf_op jit(solution)/shard_map/all_to_all | solution.py:42
  131.9 0.0 copy-done.3
  132.0 1.0 bitcast_select_fusion
  133.0 29.6 %all-to-all-done.5 = bf16[4,4,1152,128]{3,2,1,0:T(8,128)(2,1)} async-done(((bf16[4,4,1152,128]{3,2,1,0:T(8,128)(2,1)}), bf16[4,4,1152,128]{3,2,1,0:T(8,128)(2,1)}, u32[]{:S(2)}, u32[]{:S(2)}) %all-to-all-start.5) | async-done | bytes 4718624 | tf_op jit(solution)/shard_map/all_to_all | solution.py:42
  162.6 3.5 %all-to-all-start.7 = ((bf16[4,1024,128]{2,1,0:T(8,128)(2,1)}), bf16[4,1024,128]{2,1,0:T(8,128)(2,1)S(1)}, u32[]{:S(2)}, u32[]{:S(2)}) async-start(bf16[4,1024,128]{2,1,0:T(8,128)(2,1)} %bitcast.17), calls=%async_computation.7 | async-start | bytes 2097152 | tf_op jit(solution)/shard_map/all_to_all | solution.py:42
  166.1 0.5 broadcast_select_fusion.perm_ref
  166.6 9.1 %up.1 = bf16[4,1152,256]{2,1,0:T(8,128)(2,1)} custom-call(s32[16]{0:T(128)} %broadcast_select_fusion.perm_ref, bf16[16,1152,128]{2,1,0:T(8,128)(2,1)} %bitcast.11.x_ref, f32[1,2048]{1,0:T(1,128)} %bitcast.40, bf16[2048,256]{1,0:T(8,128)(2,1)} %bitcast.35, bf16[2048,256]{1,0:T(8,128)(2,1)} %bitcast.36), custom_call_target="tpu_custom_call" | custom-call | tf_op jit(solution)/shard_map/up/pallas_call | solution.py:293
  175.7 1.2 all-to-all-done.7.w_ref
  176.9 0.0 copy-start.1
  176.9 22.4 %all_to_all.59.act_ref = bf16[4,1152,256]{2,1,0:T(8,128)(2,1)} all-to-all(bf16[4,1152,256]{2,1,0:T(8,128)(2,1)} %up.1), channel_id=1, replica_groups={{0,1,2,3},{4,5,6,7},{8,9,10,11},{12,13,14,15},{16,20,24,28},{17,21,25,2..., dimensions={0} | all-to-all | bytes 4718592 | tf_op jit(solution)/shard_map/all_to_all | solution.py:42
  199.3 0.0 copy-done.1
  199.3 6.2 %down.1 = bf16[4,1152,128]{2,1,0:T(8,128)(2,1)} custom-call(bf16[4,1152,256]{2,1,0:T(8,128)(2,1)} %all_to_all.59.act_ref, bf16[4,1024,128]{2,1,0:T(8,128)(2,1)} %copy-done.1), custom_call_target="tpu_custom_call" | custom-call | tf_op jit(solution)/shard_map/down/pallas_call | solution.py:312
  205.5 15.1 %all_to_all.60 = bf16[4,1152,128]{2,1,0:T(8,128)(2,1)S(1)} all-to-all(bf16[4,1152,128]{2,1,0:T(8,128)(2,1)} %down.1), channel_id=1, replica_groups={{0,4,8,12},{1,5,9,13},{2,6,10,14},{3,7,11,15},{16,17,18,19},{20,21,22,2..., dimensions={0} | all-to-all | bytes 2359296 | tf_op jit(solution)/shard_map/all_to_all | solution.py:42
  220.6 0.3 reduce_sum.12
  220.9 4.0 %all_to_all.61 = bf16[2,576,128]{2,1,0:T(8,128)(2,1)S(1)} all-to-all(bf16[2,576,128]{2,1,0:T(8,128)(2,1)S(1)} %bitcast.32), channel_id=1, replica_groups=mesh['z'=16,'c'=2,'y'=4,'x'=4] {'c'}, dimensions={0} | all-to-all | bytes 589824 | tf_op jit(solution)/shard_map/all_to_all | solution.py:327
  224.9 0.3 copy.37
  225.2 0.1 copy.39
  225.3 25.8 %all_to_all.62.got_ref = bf16[16,72,128]{2,1,0:T(8,128)(2,1)} all-to-all(bf16[16,72,128]{2,1,0:T(8,128)(2,1)S(1)} %copy.39), channel_id=1, replica_groups=mesh['z'=16,'c'=2,'y'=4,'x'=4] {'z'}, dimensions={0} | all-to-all | bytes 589824 | tf_op jit(solution)/shard_map/all_to_all | solution.py:329
  251.1 2.4 back.1
  (3 shorter events, 0.1 us)
Async XLA Ops:
  0.0 63.2 %copy-start = (bf16[192,2048]{1,0:T(8,128)(2,1)S(1)}, bf16[192,2048]{1,0:T(8,128)(2,1)}, u32[]{:S(2)}) copy-start(bf16[192,2048]{1,0:T(8,128)(2,1)} %param.16) | copy-start | bytes 2359300
  55.7 21.0 %all-to-all-start.1 = ((bf16[16,192,128]{2,1,0:T(8,128)(2,1)}), bf16[16,192,128]{2,1,0:T(8,128)(2,1)S(1)}, u32[]{:S(2)}, u32[]{:S(2)}) async-start(bf16[16,192,128]{2,1,0:T(8,128)(2,1)} %mix.1), calls=%async_computation.1 | async-start | bytes 1572864 | tf_op jit(solution)/shard_map/all_to_all | solution.py:275
  76.7 0.9 copy-start.2
  126.9 5.1 %copy-start.3 = (bf16[1,4096,128]{2,1,0:T(8,128)(2,1)S(1)}, bf16[1,4096,128]{2,1,0:T(8,128)(2,1)}, u32[]{:S(2)}) copy-start(bf16[1,4096,128]{2,1,0:T(8,128)(2,1)} %param.31) | copy-start | bytes 3145732
  126.9 35.7 %all-to-all-start.5 = ((bf16[4,4,1152,128]{3,2,1,0:T(8,128)(2,1)}), bf16[4,4,1152,128]{3,2,1,0:T(8,128)(2,1)}, u32[]{:S(2)}, u32[]{:S(2)}) async-start(bf16[4,4,1152,128]{3,2,1,0:T(8,128)(2,1)} %broadcast_in_dim.7), calls=%async_computation.5 | async-start | bytes 9437184 | tf_op jit(solution)/shard_map/all_to_all | solution.py:42
  162.6 14.4 %all-to-all-start.7 = ((bf16[4,1024,128]{2,1,0:T(8,128)(2,1)}), bf16[4,1024,128]{2,1,0:T(8,128)(2,1)S(1)}, u32[]{:S(2)}, u32[]{:S(2)}) async-start(bf16[4,1024,128]{2,1,0:T(8,128)(2,1)} %bitcast.17), calls=%async_computation.7 | async-start | bytes 2097152 | tf_op jit(solution)/shard_map/all_to_all | solution.py:42
  176.9 22.4 %copy-start.1 = (bf16[4,1024,128]{2,1,0:T(8,128)(2,1)}, bf16[4,1024,128]{2,1,0:T(8,128)(2,1)S(1)}, u32[]{:S(2)}) copy-start(bf16[4,1024,128]{2,1,0:T(8,128)(2,1)S(1)} %all-to-all-done.7.w_ref) | copy-start | bytes 3145732

commit v2 on v1

v2 whole, which is shorter than its diff:
```python
import jax
import jax.numpy as jnp
from jax import lax
from jax.experimental import pallas as pl
from jax.experimental.pallas import tpu as pltpu
from jax.sharding import Mesh
from jax.sharding import PartitionSpec as P

F32 = jnp.float32
BF16 = jnp.bfloat16
EPS = 1e-06
CAP = 36
PAIR = 2 * CAP
Z = 16
R = 192
W = 128
D = 2048
SLOTS = 1152
SIDE = 4
TP = SIDE * SIDE
HID = 256
SP = ("z", "c")
PLANE = ("y", "x")
CYX = ("c", "y", "x")


def place(c, y, x):
    return (c * SIDE + y) * SIDE + x


FOUR = range(SIDE)
FIRST = [[place(0, y, x) for x in FOUR] for y in FOUR] + [
    [place(1, y, x) for y in FOUR] for x in FOUR
]
SECOND = [[place(0, y, x) for y in FOUR] for x in FOUR] + [
    [place(1, y, x) for x in FOUR] for y in FOUR
]


def exchange(pieces, groups):
    return lax.all_to_all(pieces, CYX, 0, 0, axis_index_groups=groups, tiled=True)


def dot(a, b, dims):
    return lax.dot_general(a, b, (dims, ((), ())), preferred_element_type=F32)


def split(a):
    high = a.astype(BF16)
    return high, (a - high.astype(F32)).astype(BF16)


def dot2(a, b, dims):
    high, low = split(a)
    return dot(high, b, dims) + dot(low, b, dims)


def dot3(a, b, dims):
    ah, al = split(a)
    bh, bl = split(b)
    return dot(ah, bh, dims) + (dot(ah, bl, dims) + dot(al, bh, dims))


def iota2(shape, dim):
    return lax.broadcasted_iota(jnp.int32, shape, dim)


def head_body(
    at_ref,
    q_hbm,
    v_hbm,
    ff_hbm,
    fb_hbm,
    jr_hbm,
    gap_hbm,
    res_hbm,
    local_ref,
    qs_ref,
    sum_ref,
    res_ref,
    q_ref,
    v_ref,
    ff_ref,
    fb_ref,
    jr_ref,
    gap_ref,
    sems,
):
    own = pl.ds(pl.multiple_of(at_ref[2] * W, W), W)
    moves = (
        (q_hbm, q_ref),
        (ff_hbm, ff_ref),
        (jr_hbm, jr_ref),
        (gap_hbm, gap_ref),
        (v_hbm, v_ref),
        (fb_hbm, fb_ref),
        (res_hbm.at[:, own], res_ref),
    )
    copies = [pltpu.make_async_copy(a, b, sems.at[k]) for k, (a, b) in enumerate(moves)]
    for copy in copies:
        copy.start()
    for copy in copies:
        copy.wait()
    q = q_ref[...].astype(F32)
    q = q * jax.nn.sigmoid(q)
    v = v_ref[...]
    row = iota2((R, R), 0)
    col = iota2((R, R), 1)
    jr = jr_ref[...]
    jc = jnp.sum(jnp.where(row == col, jr, 0.0), axis=1, keepdims=True)
    total = None
    for d, f_ref in enumerate((ff_ref, fb_ref)):
        seen = (col <= row) if d == 0 else (col >= row)
        seen_t = (row <= col) if d == 0 else (row >= col)
        key = gap_ref[d : d + 1, :] * jax.nn.sigmoid(-f_ref[...].astype(F32))
        high, low = split(jnp.log1p(-key))
        ones = seen.astype(BF16)
        sums = dot(ones, high, ((1,), (0,))) + dot(ones, low, ((1,), (0,)))
        jump_c = jnp.sum(jnp.where(seen, jr, 0.0), axis=1, keepdims=True)
        jump_r = jnp.sum(jnp.where(seen_t, jc, 0.0), axis=0, keepdims=True)
        mid = sums[R // 2 : R // 2 + 1, :]
        scores = dot3(q * jnp.exp(sums - mid), key * jnp.exp(mid - sums), ((1,), (1,)))
        fade = jnp.exp(jnp.where(seen, jump_c - jump_r, -1e30))
        part = dot2(scores * fade, v, ((1,), (0,)))
        total = part if total is None else total + part
        last = R - 1 if d == 0 else 0
        end = sums[last : last + 1, :]
        end_jump = jump_c[last : last + 1, :]
        key_end = key * jnp.exp((end - sums) + (end_jump - jump_c))
        high, low = split(key_end)
        sum_ref[d, 0:W, :] = dot(v, high, ((0,), (0,))) + dot(v, low, ((0,), (0,)))
        sum_ref[d, W : W + 8, :] = jnp.broadcast_to(jnp.exp(end + end_jump), (8, W))
        qs_ref[d] = q * jnp.exp(sums + jump_c)
    local_ref[...] = total


def pack_body(at_ref, sum_ref, out_ref):
    z = at_ref[0]
    c = at_ref[1]
    start = pl.multiple_of(c * (W // 2), W // 2)

    def message(d):
        near, far = (1, 0) if d == 0 else (0, 1)
        near_decay = sum_ref[near, d, W : W + 1, :]
        decay = sum_ref[far, d, W : W + 1, :] * near_decay
        state = (
            sum_ref[far, d, pl.ds(start, W // 2), :] * near_decay
            + sum_ref[near, d, pl.ds(start, W // 2), :]
        )
        high = decay.astype(BF16).astype(F32)
        low = decay - high
        line = iota2((8, W), 0)
        tail = jnp.where(line == 0, high, jnp.where(line == 1, low, 0.0))
        return jnp.concatenate([state, tail], axis=0).astype(BF16)

    fwd = message(0)
    bwd = message(1)
    for k in range(Z):
        later = jnp.full((W // 2 + 8, W), k, jnp.int32) > z
        out_ref[k] = jnp.where(later, fwd.astype(F32), bwd.astype(F32)).astype(BF16)


def carry_body(at_ref, got_ref, out_ref):
    z = at_ref[0]

    def step(k, carry):
        got = got_ref[k].astype(F32)
        return carry * (got[W // 2 : W // 2 + 1] + got[W // 2 + 1 : W // 2 + 2]) + got[: W // 2]

    zero = jnp.zeros((W // 2, W), F32)
    out_ref[0] = lax.fori_loop(0, z, step, zero)
    out_ref[1] = lax.fori_loop(0, Z - 1 - z, lambda k, s: step(Z - 1 - k, s), zero)


def mix_body(at_ref, local_ref, qs_ref, sum_ref, carry_ref, gate_ref, gain_ref, w_ref, out_ref):
    c = at_ref[1]
    o = local_ref[...]
    for d in range(2):
        carry = jnp.concatenate([carry_ref[0, d], carry_ref[1, d]], axis=0)
        through = carry * sum_ref[d, d, W : W + 1, :] + sum_ref[d, d, 0:W, :]
        passed = jnp.full((W, W), c, jnp.int32) != d
        o = o + dot3(qs_ref[d], jnp.where(passed, through, carry), ((1,), (1,)))
    mean_square = jnp.mean(o * o, axis=1, keepdims=True)
    gate = gate_ref[...].astype(F32)
    gated = o * lax.rsqrt(mean_square + EPS) * gain_ref[...] * (gate * jax.nn.sigmoid(gate))
    terms = dot(gated.astype(BF16), w_ref[...], ((1,), (0,))).astype(BF16)
    for k in range(TP):
        out_ref[k] = terms[:, k * W : (k + 1) * W]


def slots_of(ids, expert):
    named = ids[0:1] == expert
    for j in range(1, 4):
        named = named | (ids[j : j + 1] == expert)
    before = (iota2((R, R), 0) < iota2((R, R), 1)).astype(BF16)
    rank = dot(named.astype(BF16), before, ((1,), (0,)))
    return jnp.where(named, rank, -1000.0)


def send_body(at_ref, got_ref, res_ref, ids_ref, stream_ref, out_ref):
    total = got_ref[0].astype(F32)
    for k in range(1, TP):
        total = total + got_ref[k].astype(F32)
    stream = (res_ref[...].astype(F32) + total).astype(BF16)
    stream_ref[...] = stream
    slots = slots_of(ids_ref[...], iota2((32, R), 0))
    line = iota2((PAIR, R), 0).astype(F32)
    for z in range(Z):
        hit = (line == slots[2 * z : 2 * z + 1]) | (line == slots[2 * z + 1 : 2 * z + 2] + CAP)
        out_ref[z] = dot(hit.astype(BF16), stream, ((1,), (0,))).astype(BF16)


def pick_body(at_ref, got_ref, wg_hbm, wu_hbm, out_ref, wg_ref, wu_ref, sems):
    c = at_ref[1]
    copies = [
        pltpu.make_async_copy(wg_hbm, wg_ref, sems.at[0]),
        pltpu.make_async_copy(wu_hbm, wu_ref, sems.at[1]),
    ]
    for copy in copies:
        copy.start()
    line = iota2((PAIR, 2 * PAIR), 0)
    source = iota2((PAIR, 2 * PAIR), 1)
    wanted = line + c * CAP + jnp.where(line < CAP, 0, PAIR - CAP)
    choose = (source == wanted).astype(BF16)
    for z in range(Z):
        both = jnp.concatenate([got_ref[0, z], got_ref[1, z]], axis=0)
        rows = dot(choose, both, ((1,), (0,))).astype(BF16)
        for k in range(SIDE):
            out_ref[k, z * PAIR : (z + 1) * PAIR, :] = rows
    for copy in copies:
        copy.wait()


def fan_body(at_ref, got_ref, wd_hbm, out_ref, sems):
    turned = at_ref[1] == 1
    copies = []
    for k in range(TP):
        a, b = divmod(k, SIDE)
        source = jnp.where(turned, b * SIDE + a, k)
        rows = pl.ds(pl.multiple_of(source * HID, HID), HID)
        target = out_ref.at[a, pl.ds(SIDE * SLOTS + b * HID, HID)]
        copies.append(pltpu.make_async_copy(wd_hbm.at[rows], target, sems.at[k]))
    for copy in copies:
        copy.start()
    for k in range(SIDE):
        rows = got_ref[k]
        for other in range(SIDE):
            out_ref[other, k * SLOTS : (k + 1) * SLOTS] = rows
    for copy in copies:
        copy.wait()


def up_body(at_ref, x0_ref, x1_ref, x2_ref, x3_ref, gain_ref, wg_ref, wu_ref, out_ref, rows_ref):
    turned = at_ref[1] == 1
    parts = (x0_ref, x1_ref, x2_ref, x3_ref)
    squares = None
    for x_ref in parts:
        for a in range(SIDE):
            x = x_ref[a].astype(F32)
            squares = x * x if squares is None else squares + x * x
    scale = lax.rsqrt(jnp.sum(squares, axis=1, keepdims=True) / D + EPS)
    for b, x_ref in enumerate(parts):
        for a in range(SIDE):
            share = jnp.where(turned, b * SIDE + a, a * SIDE + b)
            cols = pl.ds(pl.multiple_of(share * W, W), W)
            x = x_ref[a].astype(F32)
            rows_ref[:, cols] = (x * scale * gain_ref[:, cols]).astype(BF16)
    rows = rows_ref[...]
    c = jnp.minimum(dot(rows, wg_ref[...], ((1,), (0,))), 7.0)
    u = jnp.clip(dot(rows, wu_ref[...], ((1,), (0,))), -7.0, 7.0)
    active = (c * jax.nn.sigmoid(1.702 * c) * (u + 1.0)).astype(BF16)
    for k in range(SIDE):
        out_ref[k] = active


def down_body(act_ref, w0_ref, w1_ref, out_ref, whole_ref):
    @pl.when(pl.program_id(0) == 0)
    def _():
        half = SIDE * HID // 2
        for k in range(SIDE):
            whole_ref[:half, k * W : (k + 1) * W] = w0_ref[k]
            whole_ref[half:, k * W : (k + 1) * W] = w1_ref[k]

    active = jnp.concatenate([act_ref[k] for k in range(SIDE)], axis=1)
    made = dot(active, whole_ref[...], ((1,), (0,))).astype(BF16)
    for k in range(SIDE):
        out_ref[k] = made[:, k * W : (k + 1) * W]


def return_body(at_ref, got_ref, stream_ref, ids_ref, weights_ref, out_ref):
    ids = ids_ref[...]
    weights = weights_ref[...]
    group = iota2((32, R), 0)
    expert = jnp.where(group < Z, 2 * group, 2 * group - 31)
    slots = slots_of(ids, expert)
    share = jnp.where(ids[0:1] == expert, weights[0:1], 0.0)
    for j in range(1, 4):
        share = share + jnp.where(ids[j : j + 1] == expert, weights[j : j + 1], 0.0)
    line = iota2((32, 32 * PAIR), 1)
    first = iota2((32, 32 * PAIR), 0) * PAIR
    inside = (line >= first) & (line < first + PAIR)
    spread = inside.astype(BF16)
    place_in = jnp.sum(jnp.where(inside, line - first, 0), axis=0, keepdims=True)
    rank = (place_in - at_ref[1] * CAP).astype(F32)
    high, low = split(share)
    slot_at = dot(slots.astype(BF16), spread, ((0,), (0,)))
    share_at = dot(high, spread, ((0,), (0,))) + dot(low, spread, ((0,), (0,)))
    mixing = jnp.where(slot_at == rank, share_at, 0.0)
    got = jnp.concatenate([got_ref[k, z] for k in range(2) for z in range(Z)], axis=0)
    total = dot2(mixing, got, ((1,), (0,)))
    out_ref[...] = (stream_ref[...].astype(F32) + total).astype(BF16)


def limit(mib):
    return pltpu.CompilerParams(vmem_limit_bytes=mib << 20)


VMEM = pl.BlockSpec()
SMEM = pl.BlockSpec(memory_space=pltpu.SMEM)
HBM = pl.BlockSpec(memory_space=pltpu.HBM)
IN_VMEM = pl.BlockSpec(memory_space=pltpu.VMEM)


def in_hbm(x):
    return pltpu.with_memory_space_constraint(x, pltpu.HBM)


def whole(body, outs, specs, name):
    return pl.pallas_call(
        body,
        out_shape=[jax.ShapeDtypeStruct(s, t) for s, t in outs],
        in_specs=specs,
        out_specs=[VMEM] * len(outs),
        compiler_params=limit(12),
        name=name,
    )


def share_of_rows(b, step):
    return pl.BlockSpec((SIDE, step, W), lambda i, p: (0, b * (SLOTS // step) + i, 0))


def shards(
    residual,
    query_in,
    value_in,
    forget_fwd,
    forget_bwd,
    jumps,
    gate_gap,
    out_gate,
    head_gain,
    out_weight,
    norm_gain,
    route_ids,
    route_weights,
    w_gate,
    w_up,
    w_down,
):
    z = lax.axis_index("z")
    c = lax.axis_index("c")
    tp = lax.axis_index(PLANE)
    at = jnp.stack([z, c, tp]).astype(jnp.int32)
    ids = route_ids.T
    weights = route_weights.T

    local, qs, summary, own_residual = pl.pallas_call(
        head_body,
        out_shape=[
            jax.ShapeDtypeStruct((R, W), F32),
            jax.ShapeDtypeStruct((2, R, W), F32),
            jax.ShapeDtypeStruct((2, W + 8, W), F32),
            jax.ShapeDtypeStruct((R, W), BF16),
        ],
        in_specs=[SMEM] + [HBM] * 7,
        out_specs=[VMEM] * 4,
        scratch_shapes=[pltpu.VMEM((R, W), BF16)] * 4
        + [pltpu.VMEM((1, R), F32), pltpu.VMEM((2, W), F32), pltpu.SemaphoreType.DMA((7,))],
        compiler_params=limit(8),
        name="head",
    )(
        at,
        *(
            in_hbm(x)
            for x in (query_in, value_in, forget_fwd, forget_bwd, jumps, gate_gap, residual)
        ),
    )
    both = lax.all_gather(summary, "c")
    (packed,) = whole(pack_body, (((Z, W // 2 + 8, W), BF16),), [SMEM, VMEM], "pack")(at, both)
    packed = lax.all_to_all(packed, "z", 0, 0, tiled=True)
    (half,) = whole(carry_body, (((2, W // 2, W), F32),), [SMEM, VMEM], "carry")(at, packed)
    carry = lax.all_gather(half, "c")
    (terms,) = whole(mix_body, (((TP, R, W), BF16),), [SMEM] + [VMEM] * 7, "mix")(
        at, local, qs, both, carry, out_gate, head_gain.reshape(1, W), out_weight
    )
    terms = lax.all_to_all(terms, PLANE, 0, 0, tiled=True)

    stream, buffer = whole(
        send_body,
        (((R, W), BF16), ((Z, PAIR, W), BF16)),
        [SMEM] + [VMEM] * 3,
        "send",
    )(at, terms, own_residual, ids)

    arrived = lax.all_to_all(buffer, "z", 0, 0, tiled=True)
    arrived = lax.all_gather(arrived, "c")
    rows, gate_w, up_w = pl.pallas_call(
        pick_body,
        out_shape=[
            jax.ShapeDtypeStruct((SIDE, SLOTS, W), BF16),
            pltpu.VMEM((D, HID), BF16),
            pltpu.VMEM((D, HID), BF16),
        ],
        in_specs=[SMEM, VMEM, HBM, HBM],
        out_specs=[VMEM, IN_VMEM, IN_VMEM],
        scratch_shapes=[pltpu.SemaphoreType.DMA((2,))],
        compiler_params=limit(12),
        name="pick",
    )(at, arrived, in_hbm(w_gate[0]), in_hbm(w_up[0]))
    rows = exchange(rows, FIRST)
    rows = pl.pallas_call(
        fan_body,
        out_shape=jax.ShapeDtypeStruct((SIDE, SIDE * (SLOTS + HID), W), BF16),
        in_specs=[SMEM, VMEM, HBM],
        out_specs=VMEM,
        scratch_shapes=[pltpu.SemaphoreType.DMA((TP,))],
        compiler_params=limit(16),
        name="fan",
    )(at, rows, in_hbm(w_down[0]))
    rows = exchange(rows, SECOND)

    step = 576
    active = pl.pallas_call(
        up_body,
        grid_spec=pltpu.PrefetchScalarGridSpec(
            num_scalar_prefetch=1,
            grid=(SLOTS // step,),
            in_specs=[
                *(share_of_rows(b, step) for b in range(SIDE)),
                pl.BlockSpec((1, D), lambda i, p: (0, 0)),
                pl.BlockSpec((D, HID), lambda i, p: (0, 0)),
                pl.BlockSpec((D, HID), lambda i, p: (0, 0)),
            ],
            out_specs=pl.BlockSpec((SIDE, step, HID), lambda i, p: (0, i, 0)),
            scratch_shapes=[pltpu.VMEM((step, D), BF16)],
        ),
        out_shape=jax.ShapeDtypeStruct((SIDE, SLOTS, HID), BF16),
        compiler_params=limit(24),
        name="up",
    )(at, rows, rows, rows, rows, norm_gain.reshape(1, D), gate_w, up_w)

    active = exchange(active, FIRST)
    made = pl.pallas_call(
        down_body,
        grid=(SLOTS // step,),
        in_specs=[
            pl.BlockSpec((SIDE, step, HID), lambda i: (0, i, 0)),
            pl.BlockSpec((SIDE, 2 * HID, W), lambda i: (0, 9, 0)),
            pl.BlockSpec((SIDE, 2 * HID, W), lambda i: (0, 10, 0)),
        ],
        out_specs=pl.BlockSpec((SIDE, step, W), lambda i: (0, i, 0)),
        out_shape=jax.ShapeDtypeStruct((SIDE, SLOTS, W), BF16),
        scratch_shapes=[pltpu.VMEM((SIDE * HID, SIDE * W), BF16)],
        compiler_params=limit(16),
        name="down",
    )(active, rows, rows)
    made = exchange(made, SECOND)
    produced = jnp.sum(made.astype(F32), axis=0).astype(BF16)

    back = lax.all_to_all(produced.reshape(Z, PAIR, W), "z", 0, 0, tiled=True)
    back = lax.all_gather(back, "c")
    (mixed,) = whole(return_body, (((R, W), BF16),), [SMEM] + [VMEM] * 4, "back")(
        at, back, stream, ids, weights
    )
    return mixed


def solution(mesh):
    finer = Mesh(mesh.devices.reshape(Z, 2, SIDE, SIDE), ("z", "c", "y", "x"))
    return jax.shard_map(
        shards,
        mesh=finer,
        in_specs=(
            P(SP, None),
            P(SP, PLANE),
            P(SP, PLANE),
            P(SP, PLANE),
            P(SP, PLANE),
            P(PLANE, SP),
            P(None, PLANE),
            P(SP, PLANE),
            P(PLANE),
            P(PLANE, None),
            P(),
            P(SP, None),
            P(SP, None),
            P(SP, None, PLANE),
            P(SP, None, PLANE),
            P(SP, None, PLANE),
        ),
        out_specs=P(SP, PLANE),
        check_vma=False,
    )
```

time: 255 us -> 223 us (0.87)
  the two profiles are of different devices: /device:TPU:2 before, /device:TPU:1 now
where the time goes in v2:
time: 223 us
  blocking collectives  200 us (90%)
  Pallas kernels  21.9 us (10%)
    all_to_all x4, blocking collectives, exchange(): lax.all_to_all(pieces, CYX, 0, 0, axis_index_groups=groups, tiled=True)  83.6 us
    all_to_all x1, blocking collectives, shards(): packed = lax.all_to_all(packed, 'z', 0, 0, tiled=True)  23.7 us
    all_to_all x1, blocking collectives, shards(): terms = lax.all_to_all(terms, PLANE, 0, 0, tiled=True)  20.4 us
    all_to_all x1, blocking collectives, shards(): arrived = lax.all_to_all(buffer, 'z', 0, 0, tiled=True)  18.8 us
    all_to_all x1, blocking collectives, shards(): back = lax.all_to_all(produced.reshape(Z, PAIR, W), 'z', 0, 0, tiled=True)  18.1 us
    all_gather x1, blocking collectives, shards(): back = lax.all_gather(back, 'c')  9.97 us
    all_gather x1, blocking collectives, shards(): arrived = lax.all_gather(arrived, 'c')  9.48 us
    all_gather x1, blocking collectives, shards(): both = lax.all_gather(summary, 'c')  8.47 us

profile of v2, /device:TPU:1, one launch (start us, length us, event | category | flops | bytes accessed | tf_op | source)
XLA Modules:
  0.0 222.7 jit_solution(11740682965573692139)
XLA Ops:
  0.0 0.0 copy-start
  0.0 0.0 copy-start.5
  0.0 0.0 copy-start.1
  0.0 0.1 pad_add_fusion.at_ref
  0.1 2.9 %head.1 = (f32[192,128]{1,0:T(8,128)S(1)}, f32[2,192,128]{2,1,0:T(8,128)S(1)}, f32[2,136,128]{2,1,0:T(8,128)S(1)}, bf16[192,128]{1,0:T(8,128)(2,1)S(1)}) custom-call(s32[3]{0:T(128)S(1)} %pad_add_fusion.at_ref, bf16[192,128]{1,0:T(8,128)(2,1)} %q_hbm.1, bf16[192,128]{1,0:T(8,128)(2,1)} %v_hbm.1, bf16[192,128]{1,0:T(8,128)(2,1)} %ff_hbm.1, ...), custom_call_target="tpu_custom_call" | custom-call | tf_op jit(solution)/shard_map/head/pallas_call | solution.py:368
  3.0 8.5 %all-gather = f32[4,136,128]{2,1,0:T(8,128)S(1)} all-gather(f32[2,136,128]{2,1,0:T(8,128)S(1)} %get-tuple-element.16), channel_id=2, replica_groups=mesh['z'=16,'c'=2,'y'=4,'x'=4] {'c'}, dimensions={0}, use_global_device_ids=true | all-gather | bytes 417792 | tf_op jit(solution)/shard_map/all_gather | solution.py:389
  11.5 0.6 pack.1
  12.1 0.0 copy-start.2
  12.1 23.7 %all_to_all.40.got_ref = bf16[16,72,128]{2,1,0:T(8,128)(2,1)S(1)} all-to-all(bf16[16,72,128]{2,1,0:T(8,128)(2,1)S(1)} %pack.1), channel_id=1, replica_groups=mesh['z'=16,'c'=2,'y'=4,'x'=4] {'z'}, dimensions={0} | all-to-all | bytes 589824 | tf_op jit(solution)/shard_map/all_to_all | solution.py:391
  35.8 0.7 carry.1
  36.5 7.8 %all-gather.1 = f32[4,64,128]{2,1,0:T(8,128)S(1)} all-gather(f32[2,64,128]{2,1,0:T(8,128)S(1)} %carry.1), channel_id=3, replica_groups=mesh['z'=16,'c'=2,'y'=4,'x'=4] {'c'}, dimensions={0}, use_global_device_ids=true | all-gather | bytes 196608 | tf_op jit(solution)/shard_map/all_gather | solution.py:393
  44.3 0.0 copy-done
  44.3 0.0 copy-done.5
  44.3 0.0 copy-done.1
  44.3 1.4 mix.1
  45.7 20.4 %all_to_all.41.got_ref = bf16[16,192,128]{2,1,0:T(8,128)(2,1)S(1)} all-to-all(bf16[16,192,128]{2,1,0:T(8,128)(2,1)S(1)} %mix.1), channel_id=1, replica_groups=mesh['z'=16,'c'=2,'y'=4,'x'=4] {'y','x'}, dimensions={0} | all-to-all | bytes 1572864 | tf_op jit(solution)/shard_map/all_to_all | solution.py:397
  66.1 0.0 copy-done.2
  66.1 1.0 send.1
  67.1 18.8 %all_to_all.42 = bf16[16,72,128]{2,1,0:T(8,128)(2,1)S(1)} all-to-all(bf16[16,72,128]{2,1,0:T(8,128)(2,1)S(1)} %get-tuple-element.18), channel_id=1, replica_groups=mesh['z'=16,'c'=2,'y'=4,'x'=4] {'z'}, dimensions={0} | all-to-all | bytes 589824 | tf_op jit(solution)/shard_map/all_to_all | solution.py:406
  85.9 9.5 %all-gather.2 = bf16[32,72,128]{2,1,0:T(8,128)(2,1)S(1)} all-gather(bf16[16,72,128]{2,1,0:T(8,128)(2,1)S(1)} %all_to_all.42), channel_id=4, replica_groups=mesh['z'=16,'c'=2,'y'=4,'x'=4] {'c'}, dimensions={0}, use_global_device_ids=true | all-gather | bytes 884736 | tf_op jit(solution)/shard_map/all_gather | solution.py:407
  95.4 2.1 pick.1
  97.5 13.2 %all_to_all.43.got_ref = bf16[4,1152,128]{2,1,0:T(8,128)(2,1)S(1)} all-to-all(bf16[4,1152,128]{2,1,0:T(8,128)(2,1)S(1)} %get-tuple-element.19), channel_id=1, replica_groups={{0,1,2,3},{4,5,6,7},{8,9,10,11},{12,13,14,15},{16,20,24,28},{17,21,25,2..., dimensions={0} | all-to-all | bytes 2359296 | tf_op jit(solution)/shard_map/all_to_all | solution.py:41
  110.7 1.9 fan.1
  112.6 0.0 copy-start.3
  112.6 37.9 %all_to_all.44.x0_ref.x1_ref.x2_ref.x3_ref.w0_ref.w1_ref = bf16[4,5632,128]{2,1,0:T(8,128)(2,1)S(1)} all-to-all(bf16[4,5632,128]{2,1,0:T(8,128)(2,1)S(1)} %fan.1), channel_id=1, replica_groups={{0,4,8,12},{1,5,9,13},{2,6,10,14},{3,7,11,15},{16,17,18,19},{20,21,22,2..., dimensions={0} | all-to-all | bytes 11534336 | tf_op jit(solution)/shard_map/all_to_all | solution.py:41
  150.6 0.0 copy-done.3
  150.6 6.4 %up.1 = bf16[4,1152,256]{2,1,0:T(8,128)(2,1)S(1)} custom-call(s32[3]{0:T(128)S(1)} %pad_add_fusion.at_ref, bf16[4,5632,128]{2,1,0:T(8,128)(2,1)S(1)} %all_to_all.44.x0_ref.x1_ref.x2_ref.x3_ref.w0_ref.w1_ref, bf16[4,5632,128]{2,1,0:T(8,128)(2,1)S(1)} %all_to_all.44.x0_ref.x1_ref.x2_ref.x3_ref.w0_ref.w1_ref, ...), custom_call_target="tpu_custom_call" | custom-call | tf_op jit(solution)/shard_map/up/pallas_call | solution.py:434
  156.9 19.3 %all_to_all.45.act_ref = bf16[4,1152,256]{2,1,0:T(8,128)(2,1)S(1)} all-to-all(bf16[4,1152,256]{2,1,0:T(8,128)(2,1)S(1)} %up.1), channel_id=1, replica_groups={{0,1,2,3},{4,5,6,7},{8,9,10,11},{12,13,14,15},{16,20,24,28},{17,21,25,2..., dimensions={0} | all-to-all | bytes 4718592 | tf_op jit(solution)/shard_map/all_to_all | solution.py:41
  176.3 2.1 down.1
  178.4 0.0 copy-start.4
  178.4 13.2 %all_to_all.46 = bf16[4,1152,128]{2,1,0:T(8,128)(2,1)S(1)} all-to-all(bf16[4,1152,128]{2,1,0:T(8,128)(2,1)S(1)} %down.1), channel_id=1, replica_groups={{0,4,8,12},{1,5,9,13},{2,6,10,14},{3,7,11,15},{16,17,18,19},{20,21,22,2..., dimensions={0} | all-to-all | bytes 2359296 | tf_op jit(solution)/shard_map/all_to_all | solution.py:41
  191.5 0.3 reduce_sum.12
  191.9 18.1 %all_to_all.47 = bf16[16,72,128]{2,1,0:T(8,128)(2,1)S(1)} all-to-all(bf16[16,72,128]{2,1,0:T(8,128)(2,1)S(1)} %bitcast.25), channel_id=1, replica_groups=mesh['z'=16,'c'=2,'y'=4,'x'=4] {'z'}, dimensions={0} | all-to-all | bytes 589824 | tf_op jit(solution)/shard_map/all_to_all | solution.py:471
  210.0 10.0 %all-gather.3 = bf16[32,72,128]{2,1,0:T(8,128)(2,1)S(1)} all-gather(bf16[16,72,128]{2,1,0:T(8,128)(2,1)S(1)} %all_to_all.47), channel_id=5, replica_groups=mesh['z'=16,'c'=2,'y'=4,'x'=4] {'c'}, dimensions={0}, use_global_device_ids=true | all-gather | bytes 884736 | tf_op jit(solution)/shard_map/all_gather | solution.py:472
  219.9 0.0 copy-done.4
  219.9 2.8 %back.1 = bf16[192,128]{1,0:T(8,128)(2,1)} custom-call(s32[3]{0:T(128)S(1)} %pad_add_fusion.at_ref, bf16[2,16,72,128]{3,2,1,0:T(8,128)(2,1)S(1)} %bitcast.17, bf16[192,128]{1,0:T(8,128)(2,1)S(1)} %get-tuple-element.22.stream_ref, s32[4,192]{1,0:T(4,128)S(1)} %bitcast.21, f32[4,192]{1,0:T(4,128)S(1)} %bitcast.23), custom_call_target="tpu_custom_call" | custom-call | tf_op jit(solution)/shard_map/back/pallas_call | solution.py:473
Async XLA Ops:
  0.0 44.3 %copy-start = (bf16[128,2048]{1,0:T(8,128)(2,1)S(1)}, bf16[128,2048]{1,0:T(8,128)(2,1)}, u32[]{:S(2)}) copy-start(bf16[128,2048]{1,0:T(8,128)(2,1)} %w_ref.1) | copy-start | bytes 1572868
  0.0 44.3 %copy-start.5 = (f32[128]{0:T(128)S(1)}, f32[128]{0:T(128)}, u32[]{:S(2)}) copy-start(f32[128]{0:T(128)} %param.24) | copy-start | bytes 1540
  0.0 44.3 %copy-start.1 = (bf16[192,128]{1,0:T(8,128)(2,1)S(1)}, bf16[192,128]{1,0:T(8,128)(2,1)}, u32[]{:S(2)}) copy-start(bf16[192,128]{1,0:T(8,128)(2,1)} %gate_ref.1) | copy-start | bytes 147460
  12.1 54.0 %copy-start.2 = (s32[192,4]{0,1:T(4,128)S(1)}, s32[192,4]{0,1:T(4,128)}, u32[]{:S(2)}) copy-start(s32[192,4]{0,1:T(4,128)} %param.27) | copy-start | bytes 9220
  112.6 38.0 %copy-start.3 = (f32[2048]{0:T(1024)S(1)}, f32[2048]{0:T(1024)}, u32[]{:S(2)}) copy-start(f32[2048]{0:T(1024)} %param.26) | copy-start | bytes 24580
  178.4 41.6 %copy-start.4 = (f32[192,4]{0,1:T(4,128)S(1)}, f32[192,4]{0,1:T(4,128)}, u32[]{:S(2)}) copy-start(f32[192,4]{0,1:T(4,128)} %param.28) | copy-start | bytes 9220

commit v3 on v2

--- a/solution.py
+++ b/solution.py
@@ -16,6 +16,7 @@
 W = 128
 D = 2048
 SLOTS = 1152
+PART = 288
 SIDE = 4
 TP = SIDE * SIDE
 HID = 256
@@ -39,6 +40,19 @@
 
 def exchange(pieces, groups):
     return lax.all_to_all(pieces, CYX, 0, 0, axis_index_groups=groups, tiled=True)
+
+
+def ring(step):
+    return [
+        (place(c, y, x), place(c, (y + step * c) % SIDE, (x + step * (1 - c)) % SIDE))
+        for c in range(2)
+        for y in FOUR
+        for x in FOUR
+    ]
+
+
+def passed_on(x, step):
+    return lax.ppermute(x, CYX, ring(step))
 
 
 def dot(a, b, dims):
@@ -74,10 +88,15 @@
     jr_hbm,
     gap_hbm,
     res_hbm,
+    wg_hbm,
+    wu_hbm,
+    wd_hbm,
     local_ref,
     qs_ref,
     sum_ref,
     res_ref,
+    joined_hbm,
+    held_ref,
     q_ref,
     v_ref,
     ff_ref,
@@ -97,10 +116,21 @@
         (res_hbm.at[:, own], res_ref),
     )
     copies = [pltpu.make_async_copy(a, b, sems.at[k]) for k, (a, b) in enumerate(moves)]
-    for copy in copies:
+    inward = []
+    outward = []
+    for k, w_hbm in enumerate((wg_hbm, wg_hbm, wu_hbm, wu_hbm, wd_hbm)):
+        source = w_hbm if k == 4 else w_hbm.at[:, pl.ds((k % 2) * W, W)]
+        held = held_ref.at[pl.ds(k * D, 2 * D if k == 4 else D)]
+        target = joined_hbm.at[pl.ds(k * D, 2 * D if k == 4 else D)]
+        inward.append(pltpu.make_async_copy(source, held, sems.at[7 + k]))
+        outward.append(pltpu.make_async_copy(held, target, sems.at[12 + k]))
+    for copy in copies + inward:
         copy.start()
     for copy in copies:
         copy.wait()
+    for first, second in zip(inward, outward):
+        first.wait()
+        second.start()
     q = q_ref[...].astype(F32)
     q = q * jax.nn.sigmoid(q)
     v = v_ref[...]
@@ -132,6 +162,8 @@
         sum_ref[d, W : W + 8, :] = jnp.broadcast_to(jnp.exp(end + end_jump), (8, W))
         qs_ref[d] = q * jnp.exp(sums + jump_c)
     local_ref[...] = total
+    for copy in outward:
+        copy.wait()
 
 
 def pack_body(at_ref, sum_ref, out_ref):
@@ -210,81 +242,76 @@
         out_ref[z] = dot(hit.astype(BF16), stream, ((1,), (0,))).astype(BF16)
 
 
-def pick_body(at_ref, got_ref, wg_hbm, wu_hbm, out_ref, wg_ref, wu_ref, sems):
+def pick_body(at_ref, got_ref, out_ref):
     c = at_ref[1]
-    copies = [
-        pltpu.make_async_copy(wg_hbm, wg_ref, sems.at[0]),
-        pltpu.make_async_copy(wu_hbm, wu_ref, sems.at[1]),
-    ]
-    for copy in copies:
-        copy.start()
     line = iota2((PAIR, 2 * PAIR), 0)
     source = iota2((PAIR, 2 * PAIR), 1)
     wanted = line + c * CAP + jnp.where(line < CAP, 0, PAIR - CAP)
     choose = (source == wanted).astype(BF16)
     for z in range(Z):
         both = jnp.concatenate([got_ref[0, z], got_ref[1, z]], axis=0)
-        rows = dot(choose, both, ((1,), (0,))).astype(BF16)
-        for k in range(SIDE):
-            out_ref[k, z * PAIR : (z + 1) * PAIR, :] = rows
-    for copy in copies:
-        copy.wait()
-
-
-def fan_body(at_ref, got_ref, wd_hbm, out_ref, sems):
-    turned = at_ref[1] == 1
+        out_ref[z * PAIR : (z + 1) * PAIR, :] = dot(choose, both, ((1,), (0,))).astype(BF16)
+
+
+def up_body(
+    at_ref, x_ref, gain_ref, own, plus, minus, far0, far1, out_ref, wd_ref, w_ref, rows_ref, sems
+):
+    def piece(q, k, rows):
+        start = k * D
+        if q < 3:
+            return (own, plus, minus)[q].at[pl.ds(start, rows)]
+        return (far0, far1)[start // (3 * D)].at[pl.ds(start % (3 * D), rows)]
+
     copies = []
-    for k in range(TP):
-        a, b = divmod(k, SIDE)
-        source = jnp.where(turned, b * SIDE + a, k)
-        rows = pl.ds(pl.multiple_of(source * HID, HID), HID)
-        target = out_ref.at[a, pl.ds(SIDE * SLOTS + b * HID, HID)]
-        copies.append(pltpu.make_async_copy(wd_hbm.at[rows], target, sems.at[k]))
+    for q in range(SIDE):
+        for k in range(4):
+            target = w_ref.at[q, k // 2, :, pl.ds((k % 2) * W, W)]
+            copies.append(pltpu.make_async_copy(piece(q, k, D), target, sems.at[5 * q + k]))
+    for q in range(SIDE):
+        target = wd_ref.at[:, pl.ds(q * W, W)]
+        copies.append(pltpu.make_async_copy(piece(q, 4, 2 * D), target, sems.at[5 * q + 4]))
     for copy in copies:
         copy.start()
-    for k in range(SIDE):
-        rows = got_ref[k]
-        for other in range(SIDE):
-            out_ref[other, k * SLOTS : (k + 1) * SLOTS] = rows
-    for copy in copies:
+    turned = at_ref[1] == 1
+    squares = None
+    for p in range(TP):
+        x = x_ref[p].astype(F32)
+        squares = x * x if squares is None else squares + x * x
+    scale = lax.rsqrt(jnp.sum(squares, axis=1, keepdims=True) / D + EPS)
+    for p in range(TP):
+        share = jnp.where(turned, (p % SIDE) * SIDE + p // SIDE, p)
+        cols = pl.ds(pl.multiple_of(share * W, W), W)
+        rows_ref[:, cols] = (x_ref[p].astype(F32) * scale * gain_ref[:, cols]).astype(BF16)
+    rows = rows_ref[...]
+    for q in range(SIDE):
+        for copy in copies[4 * q : 4 * q + 4]:
+            copy.wait()
+        c = jnp.minimum(dot(rows, w_ref[q, 0], ((1,), (0,))), 7.0)
+        u = jnp.clip(dot(rows, w_ref[q, 1], ((1,), (0,))), -7.0, 7.0)
+        active = (c * jax.nn.sigmoid(1.702 * c) * (u + 1.0)).astype(BF16)
+        for k in range(SIDE):
+            out_ref[k, :, q * HID : (q + 1) * HID] = active
+    for copy in copies[4 * SIDE :]:
         copy.wait()
 
 
-def up_body(at_ref, x0_ref, x1_ref, x2_ref, x3_ref, gain_ref, wg_ref, wu_ref, out_ref, rows_ref):
-    turned = at_ref[1] == 1
-    parts = (x0_ref, x1_ref, x2_ref, x3_ref)
-    squares = None
-    for x_ref in parts:
-        for a in range(SIDE):
-            x = x_ref[a].astype(F32)
-            squares = x * x if squares is None else squares + x * x
-    scale = lax.rsqrt(jnp.sum(squares, axis=1, keepdims=True) / D + EPS)
-    for b, x_ref in enumerate(parts):
-        for a in range(SIDE):
-            share = jnp.where(turned, b * SIDE + a, a * SIDE + b)
-            cols = pl.ds(pl.multiple_of(share * W, W), W)
-            x = x_ref[a].astype(F32)
-            rows_ref[:, cols] = (x * scale * gain_ref[:, cols]).astype(BF16)
-    rows = rows_ref[...]
-    c = jnp.minimum(dot(rows, wg_ref[...], ((1,), (0,))), 7.0)
-    u = jnp.clip(dot(rows, wu_ref[...], ((1,), (0,))), -7.0, 7.0)
-    active = (c * jax.nn.sigmoid(1.702 * c) * (u + 1.0)).astype(BF16)
-    for k in range(SIDE):
-        out_ref[k] = active
-
-
-def down_body(act_ref, w0_ref, w1_ref, out_ref, whole_ref):
-    @pl.when(pl.program_id(0) == 0)
-    def _():
-        half = SIDE * HID // 2
-        for k in range(SIDE):
-            whole_ref[:half, k * W : (k + 1) * W] = w0_ref[k]
-            whole_ref[half:, k * W : (k + 1) * W] = w1_ref[k]
-
-    active = jnp.concatenate([act_ref[k] for k in range(SIDE)], axis=1)
-    made = dot(active, whole_ref[...], ((1,), (0,))).astype(BF16)
-    for k in range(SIDE):
-        out_ref[k] = made[:, k * W : (k + 1) * W]
+def along(at_ref, q):
+    a = jnp.where(at_ref[1] == 0, at_ref[2] % SIDE, at_ref[2] // SIDE)
+    return (a + (0, SIDE - 1, 1, 2)[q]) % SIDE
+
+
+def down_body(at_ref, act_ref, w_ref, out_ref):
+    made = None
+    for q in range(SIDE):
+        a = along(at_ref, q)
+        for b in range(SIDE):
+            share = jnp.where(at_ref[1] == 0, b * SIDE + a, a * SIDE + b)
+            w = w_ref[pl.ds(pl.multiple_of(share * HID, HID), HID), :]
+            term = dot(act_ref[b, :, q * HID : (q + 1) * HID], w, ((1,), (0,)))
+            made = term if made is None else made + term
+    made = made.astype(BF16)
+    for q in range(SIDE):
+        out_ref[along(at_ref, q)] = made[:, q * W : (q + 1) * W]
 
 
 def return_body(at_ref, got_ref, stream_ref, ids_ref, weights_ref, out_ref):
@@ -325,19 +352,14 @@
     return pltpu.with_memory_space_constraint(x, pltpu.HBM)
 
 
-def whole(body, outs, specs, name):
+def whole(body, outs, specs):
     return pl.pallas_call(
         body,
         out_shape=[jax.ShapeDtypeStruct(s, t) for s, t in outs],
         in_specs=specs,
         out_specs=[VMEM] * len(outs),
         compiler_params=limit(12),
-        name=name,
-    )
-
-
-def share_of_rows(b, step):
-    return pl.BlockSpec((SIDE, step, W), lambda i, p: (0, b * (SLOTS // step) + i, 0))
+    )
 
 
 def shards(
@@ -365,112 +387,94 @@
     ids = route_ids.T
     weights = route_weights.T
 
-    local, qs, summary, own_residual = pl.pallas_call(
+    local, qs, summary, own_residual, joined = pl.pallas_call(
         head_body,
         out_shape=[
             jax.ShapeDtypeStruct((R, W), F32),
             jax.ShapeDtypeStruct((2, R, W), F32),
             jax.ShapeDtypeStruct((2, W + 8, W), F32),
             jax.ShapeDtypeStruct((R, W), BF16),
+            pltpu.HBM((6 * D, W), BF16),
         ],
-        in_specs=[SMEM] + [HBM] * 7,
-        out_specs=[VMEM] * 4,
-        scratch_shapes=[pltpu.VMEM((R, W), BF16)] * 4
-        + [pltpu.VMEM((1, R), F32), pltpu.VMEM((2, W), F32), pltpu.SemaphoreType.DMA((7,))],
+        in_specs=[SMEM] + [HBM] * 10,
+        out_specs=[VMEM] * 4 + [HBM],
+        scratch_shapes=[pltpu.VMEM((6 * D, W), BF16)]
+        + [pltpu.VMEM((R, W), BF16)] * 4
+        + [pltpu.VMEM((1, R), F32), pltpu.VMEM((2, W), F32), pltpu.SemaphoreType.DMA((17,))],
         compiler_params=limit(8),
         name="head",
     )(
         at,
         *(
             in_hbm(x)
-            for x in (query_in, value_in, forget_fwd, forget_bwd, jumps, gate_gap, residual)
+            for x in (
+                query_in,
+                value_in,
+                forget_fwd,
+                forget_bwd,
+                jumps,
+                gate_gap,
+                residual,
+                w_gate[0],
+                w_up[0],
+                w_down[0],
+            )
         ),
     )
+    plus = passed_on(joined, 1)
+    minus = passed_on(joined, SIDE - 1)
     both = lax.all_gather(summary, "c")
-    (packed,) = whole(pack_body, (((Z, W // 2 + 8, W), BF16),), [SMEM, VMEM], "pack")(at, both)
+    (packed,) = whole(pack_body, (((Z, W // 2 + 8, W), BF16),), [SMEM, VMEM])(at, both)
     packed = lax.all_to_all(packed, "z", 0, 0, tiled=True)
-    (half,) = whole(carry_body, (((2, W // 2, W), F32),), [SMEM, VMEM], "carry")(at, packed)
+    (half,) = whole(carry_body, (((2, W // 2, W), F32),), [SMEM, VMEM])(at, packed)
     carry = lax.all_gather(half, "c")
-    (terms,) = whole(mix_body, (((TP, R, W), BF16),), [SMEM] + [VMEM] * 7, "mix")(
+    (terms,) = whole(mix_body, (((TP, R, W), BF16),), [SMEM] + [VMEM] * 7)(
         at, local, qs, both, carry, out_gate, head_gain.reshape(1, W), out_weight
     )
     terms = lax.all_to_all(terms, PLANE, 0, 0, tiled=True)
 
     stream, buffer = whole(
-        send_body,
-        (((R, W), BF16), ((Z, PAIR, W), BF16)),
-        [SMEM] + [VMEM] * 3,
-        "send",
+        send_body, (((R, W), BF16), ((Z, PAIR, W), BF16)), [SMEM] + [VMEM] * 3
     )(at, terms, own_residual, ids)
 
+    buffer, plus, minus = lax.optimization_barrier((buffer, plus, minus))
+    far0 = passed_on(plus[: 3 * D], 1)
+    far1 = passed_on(minus[3 * D :], SIDE - 1)
     arrived = lax.all_to_all(buffer, "z", 0, 0, tiled=True)
     arrived = lax.all_gather(arrived, "c")
-    rows, gate_w, up_w = pl.pallas_call(
-        pick_body,
+    (rows,) = whole(pick_body, (((SLOTS, W), BF16),), [SMEM, VMEM])(at, arrived)
+    rows = exchange(rows.reshape(SIDE, PART, W), FIRST)
+    rows, far0, far1 = lax.optimization_barrier((rows, far0, far1))
+    rows = exchange(jnp.broadcast_to(rows, (SIDE, *rows.shape)), SECOND).reshape(TP, PART, W)
+
+    active, down = pl.pallas_call(
+        up_body,
         out_shape=[
-            jax.ShapeDtypeStruct((SIDE, SLOTS, W), BF16),
-            pltpu.VMEM((D, HID), BF16),
-            pltpu.VMEM((D, HID), BF16),
+            jax.ShapeDtypeStruct((SIDE, PART, SIDE * HID), BF16),
+            pltpu.VMEM((2 * D, SIDE * W), BF16),
         ],
-        in_specs=[SMEM, VMEM, HBM, HBM],
-        out_specs=[VMEM, IN_VMEM, IN_VMEM],
-        scratch_shapes=[pltpu.SemaphoreType.DMA((2,))],
-        compiler_params=limit(12),
-        name="pick",
-    )(at, arrived, in_hbm(w_gate[0]), in_hbm(w_up[0]))
-    rows = exchange(rows, FIRST)
-    rows = pl.pallas_call(
-        fan_body,
-        out_shape=jax.ShapeDtypeStruct((SIDE, SIDE * (SLOTS + HID), W), BF16),
-        in_specs=[SMEM, VMEM, HBM],
-        out_specs=VMEM,
-        scratch_shapes=[pltpu.SemaphoreType.DMA((TP,))],
-        compiler_params=limit(16),
-        name="fan",
-    )(at, rows, in_hbm(w_down[0]))
-    rows = exchange(rows, SECOND)
-
-    step = 576
-    active = pl.pallas_call(
-        up_body,
-        grid_spec=pltpu.PrefetchScalarGridSpec(
-            num_scalar_prefetch=1,
-            grid=(SLOTS // step,),
-            in_specs=[
-                *(share_of_rows(b, step) for b in range(SIDE)),
-                pl.BlockSpec((1, D), lambda i, p: (0, 0)),
-                pl.BlockSpec((D, HID), lambda i, p: (0, 0)),
-                pl.BlockSpec((D, HID), lambda i, p: (0, 0)),
-            ],
-            out_specs=pl.BlockSpec((SIDE, step, HID), lambda i, p: (0, i, 0)),
-            scratch_shapes=[pltpu.VMEM((step, D), BF16)],
-        ),
-        out_shape=jax.ShapeDtypeStruct((SIDE, SLOTS, HID), BF16),
+        in_specs=[SMEM, VMEM, VMEM] + [HBM] * 5,
+        out_specs=[VMEM, IN_VMEM],
+        scratch_shapes=[
+            pltpu.VMEM((SIDE, 2, D, HID), BF16),
+            pltpu.VMEM((PART, D), BF16),
+            pltpu.SemaphoreType.DMA((5 * SIDE,)),
+        ],
         compiler_params=limit(24),
         name="up",
-    )(at, rows, rows, rows, rows, norm_gain.reshape(1, D), gate_w, up_w)
-
-    active = exchange(active, FIRST)
-    made = pl.pallas_call(
-        down_body,
-        grid=(SLOTS // step,),
-        in_specs=[
-            pl.BlockSpec((SIDE, step, HID), lambda i: (0, i, 0)),
-            pl.BlockSpec((SIDE, 2 * HID, W), lambda i: (0, 9, 0)),
-            pl.BlockSpec((SIDE, 2 * HID, W), lambda i: (0, 10, 0)),
-        ],
-        out_specs=pl.BlockSpec((SIDE, step, W), lambda i: (0, i, 0)),
-        out_shape=jax.ShapeDtypeStruct((SIDE, SLOTS, W), BF16),
-        scratch_shapes=[pltpu.VMEM((SIDE * HID, SIDE * W), BF16)],
-        compiler_params=limit(16),
-        name="down",
-    )(active, rows, rows)
-    made = exchange(made, SECOND)
-    produced = jnp.sum(made.astype(F32), axis=0).astype(BF16)
+    )(
+        at,
+        rows,
+        norm_gain.reshape(1, D),
+        *(in_hbm(w) for w in (joined, plus, minus, far0, far1)),
+    )
+    active = exchange(active, SECOND)
+    (made,) = whole(down_body, (((SIDE, PART, W), BF16),), [SMEM, VMEM, VMEM])(at, active, down)
+    produced = exchange(made, FIRST)
 
     back = lax.all_to_all(produced.reshape(Z, PAIR, W), "z", 0, 0, tiled=True)
     back = lax.all_gather(back, "c")
-    (mixed,) = whole(return_body, (((R, W), BF16),), [SMEM] + [VMEM] * 4, "back")(
+    (mixed,) = whole(return_body, (((R, W), BF16),), [SMEM] + [VMEM] * 4)(
         at, back, stream, ids, weights
     )
     return mixed

time: 223 us -> 202 us (0.906)
  blocking collectives: 200 us -> 166 us
  starting transfers between devices: 0 us -> 12.7 us
  local copies, waits for them, and re-layouts: 0.03 us -> 2.95 us
  Pallas kernels: 21.9 us -> 19.5 us
    all_to_all x4, blocking collectives: 83.6 us -> 48.8 us  [exchange(): lax.all_to_all(pieces, CYX, 0, 0, axis_index_groups=groups, tiled=True)]
    ppermute x0 -> x4, starting transfers between devices: none -> 12.7 us  [passed_on(): return lax.ppermute(x, CYX, ring(step))]
    pallas_call x8 -> x7, Pallas kernels: 17.9 us -> 14.3 us  [the longest x1 6.08 us: shards(): pl.pallas_call(up_body, out_shape=[jax.ShapeDtypeStruct((SIDE, PART, SIDE...]
    unnamed x12 -> x20, local copies, waits for them, and re-layouts: 0.03 us -> 2.59 us
  transfers between devices with their start and end apart: 0 -> 4, of which waited for: 0 -> 0; matrix products, arithmetic and copies ran while one was open for 0% -> 0% of each run, Pallas kernels for 0% -> 2%
where the time goes in v3:
time: 202 us; the launch traced here: 201 us
  blocking collectives  166 us (82%)
  Pallas kernels  19.5 us (10%)
  starting transfers between devices  12.7 us (6%)
  local copies, waits for them, and re-layouts  2.95 us (1%)
    all_to_all x4, blocking collectives, exchange(): lax.all_to_all(pieces, CYX, 0, 0, axis_index_groups=groups, tiled=True)  48.8 us
    all_to_all x1, blocking collectives, shards(): packed = lax.all_to_all(packed, 'z', 0, 0, tiled=True)  24.5 us
    all_to_all x1, blocking collectives, shards(): terms = lax.all_to_all(terms, PLANE, 0, 0, tiled=True)  20.6 us
    all_to_all x1, blocking collectives, shards(): back = lax.all_to_all(produced.reshape(Z, PAIR, W), 'z', 0, 0, tiled=True)  19 us
    all_to_all x1, blocking collectives, shards(): arrived = lax.all_to_all(buffer, 'z', 0, 0, tiled=True)  18.5 us
    ppermute x4, starting transfers between devices, passed_on(): return lax.ppermute(x, CYX, ring(step))  12.7 us
    all_gather x1, blocking collectives, shards(): back = lax.all_gather(back, 'c')  10 us
    all_gather x1, blocking collectives, shards(): arrived = lax.all_gather(arrived, 'c')  9.67 us
  transfers between devices with their start and end apart: 4, of which 0 were waited for; matrix products, arithmetic and copies ran while one was open for 0% of the time, Pallas kernels for 2%

profile of v3, /device:TPU:1, one launch (start us, length us, event | category | flops | bytes accessed | tf_op | source)
XLA Modules:
  0.0 201.1 jit_solution(14685984154269805425)
XLA Ops:
  0.0 0.1 pad_add_fusion.at_ref
  0.1 0.0 copy-start
  0.1 0.0 copy-start.1
  0.1 0.0 copy-start.5
  0.1 4.1 %head.1 = (f32[192,128]{1,0:T(8,128)S(1)}, f32[2,192,128]{2,1,0:T(8,128)S(1)}, f32[2,136,128]{2,1,0:T(8,128)S(1)}, bf16[192,128]{1,0:T(8,128)(2,1)S(1)}, bf16[12288,128]{1,0:T(8,128)(2,1)}) custom-call(s32[3]{0:T(128)S(1)} %pad_add_fusion.at_ref, bf16[192,128]{1,0:T(8,128)(2,1)} %q_hbm.1, bf16[192,128]{1,0:T(8,128)(2,1)} %v_hbm.1, bf16[192,128]{1,0:T(8,128)(2,1)} %ff_hbm.1, ...), custom_call_target="tpu_custom_call" | custom-call | tf_op jit(solution)/shard_map/head/pallas_call | solution.py:390
  4.2 5.5 %collective-permute-start.1 = (bf16[12288,128]{1,0:T(8,128)(2,1)}, bf16[12288,128]{1,0:T(8,128)(2,1)S(1)}, u32[]{:S(2)}, u32[]{:S(2)}) collective-permute-start(bf16[12288,128]{1,0:T(8,128)(2,1)} %get-tuple-element.25.own), channel_id=1, source_target_pairs={{0,3},{1,0},{2,1},{3,2},{4,7},{5,4},{6,5},{7,6},{8,11},{9,8},{10,9... | collective-permute-start | bytes 9437192 | tf_op jit(solution)/shard_map/ppermute | solution.py:55
  9.7 1.9 collective-permute-start
  11.6 6.9 %all-gather = f32[4,136,128]{2,1,0:T(8,128)S(1)} all-gather(f32[2,136,128]{2,1,0:T(8,128)S(1)} %get-tuple-element.22), channel_id=2, replica_groups=mesh['z'=16,'c'=2,'y'=4,'x'=4] {'c'}, dimensions={0}, use_global_device_ids=true | all-gather | bytes 417792 | tf_op jit(solution)/shard_map/all_gather | solution.py:426
  18.6 0.6 shard_map.154
  19.1 0.0 copy-start.2
  19.2 24.5 %all_to_all.40.got_ref = bf16[16,72,128]{2,1,0:T(8,128)(2,1)S(1)} all-to-all(bf16[16,72,128]{2,1,0:T(8,128)(2,1)S(1)} %shard_map.154), channel_id=1, replica_groups=mesh['z'=16,'c'=2,'y'=4,'x'=4] {'z'}, dimensions={0} | all-to-all | bytes 589824 | tf_op jit(solution)/shard_map/all_to_all | solution.py:428
  43.6 0.7 shard_map.155
  44.3 7.8 %all-gather.1 = f32[4,64,128]{2,1,0:T(8,128)S(1)} all-gather(f32[2,64,128]{2,1,0:T(8,128)S(1)} %shard_map.155), channel_id=3, replica_groups=mesh['z'=16,'c'=2,'y'=4,'x'=4] {'c'}, dimensions={0}, use_global_device_ids=true | all-gather | bytes 196608 | tf_op jit(solution)/shard_map/all_gather | solution.py:430
  52.1 0.0 copy-done
  52.1 0.0 copy-done.1
  52.1 0.0 copy-done.5
  52.1 1.4 shard_map.156
  53.5 20.6 %all_to_all.41.got_ref = bf16[16,192,128]{2,1,0:T(8,128)(2,1)S(1)} all-to-all(bf16[16,192,128]{2,1,0:T(8,128)(2,1)S(1)} %shard_map.156), channel_id=1, replica_groups=mesh['z'=16,'c'=2,'y'=4,'x'=4] {'y','x'}, dimensions={0} | all-to-all | bytes 1572864 | tf_op jit(solution)/shard_map/all_to_all | solution.py:434
  74.1 0.0 copy-done.2
  74.1 1.0 shard_map.157
  75.1 0.0 collective-permute-done.1.minus
  75.1 0.0 copy-start.6
  75.2 0.0 collective-permute-done.plus
  75.2 0.0 copy-start.7
  75.2 0.1 slice.6
  75.3 0.1 slice.7
  75.4 1.5 copy-done.6
  76.9 1.1 copy-done.7
  77.9 2.5 %collective-permute-start.3 = (bf16[6144,128]{1,0:T(8,128)(2,1)S(1)}, bf16[6144,128]{1,0:T(8,128)(2,1)S(1)}, u32[]{:S(2)}, u32[]{:S(2)}) collective-permute-start(bf16[6144,128]{1,0:T(8,128)(2,1)S(1)} %slice.7), channel_id=1, source_target_pairs={{0,3},{1,0},{2,1},{3,2},{4,7},{5,4},{6,5},{7,6},{8,11},{9,8},{10,9... | collective-permute-start | bytes 4718600 | tf_op jit(solution)/shard_map/ppermute | solution.py:55
  80.4 2.8 %collective-permute-start.2 = (bf16[6144,128]{1,0:T(8,128)(2,1)S(1)}, bf16[6144,128]{1,0:T(8,128)(2,1)S(1)}, u32[]{:S(2)}, u32[]{:S(2)}) collective-permute-start(bf16[6144,128]{1,0:T(8,128)(2,1)S(1)} %slice.6), channel_id=1, source_target_pairs={{0,1},{1,2},{2,3},{3,0},{4,5},{5,6},{6,7},{7,4},{8,9},{9,10},{10,1... | collective-permute-start | bytes 4718600 | tf_op jit(solution)/shard_map/ppermute | solution.py:55
  83.2 18.5 %all_to_all.42 = bf16[16,72,128]{2,1,0:T(8,128)(2,1)S(1)} all-to-all(bf16[16,72,128]{2,1,0:T(8,128)(2,1)S(1)} %get-tuple-element.26), channel_id=1, replica_groups=mesh['z'=16,'c'=2,'y'=4,'x'=4] {'z'}, dimensions={0} | all-to-all | bytes 589824 | tf_op jit(solution)/shard_map/all_to_all | solution.py:443
  101.7 9.7 %all-gather.2 = bf16[32,72,128]{2,1,0:T(8,128)(2,1)S(1)} all-gather(bf16[16,72,128]{2,1,0:T(8,128)(2,1)S(1)} %all_to_all.42), channel_id=4, replica_groups=mesh['z'=16,'c'=2,'y'=4,'x'=4] {'c'}, dimensions={0}, use_global_device_ids=true | all-gather | bytes 884736 | tf_op jit(solution)/shard_map/all_gather | solution.py:444
  111.4 0.9 shard_map.158
  112.3 0.0 copy-start.3
  112.3 8.3 %all_to_all.43 = bf16[4,288,128]{2,1,0:T(8,128)(2,1)S(1)} all-to-all(bf16[4,288,128]{2,1,0:T(8,128)(2,1)S(1)} %bitcast.22), channel_id=1, replica_groups={{0,1,2,3},{4,5,6,7},{8,9,10,11},{12,13,14,15},{16,20,24,28},{17,21,25,2..., dimensions={0} | all-to-all | bytes 589824 | tf_op jit(solution)/shard_map/all_to_all | solution.py:42
  120.6 0.0 collective-permute-done.3.far1
  120.6 0.0 copy-start.8
  120.6 0.0 collective-permute-done.2.far0
  120.6 0.0 copy-start.9
  120.6 0.2 broadcast_in_dim.3
  120.8 13.2 %all_to_all.44 = bf16[4,4,288,128]{3,2,1,0:T(8,128)(2,1)S(1)} all-to-all(bf16[4,4,288,128]{3,2,1,0:T(8,128)(2,1)S(1)} %broadcast_in_dim.3), channel_id=1, replica_groups={{0,4,8,12},{1,5,9,13},{2,6,10,14},{3,7,11,15},{16,17,18,19},{20,21,22,2..., dimensions={0} | all-to-all | bytes 2359296 | tf_op jit(solution)/shard_map/all_to_all | solution.py:42
  134.0 0.0 copy-done.8
  134.0 0.0 copy-done.9
  134.0 0.0 copy-done.3
  134.0 6.1 %up.1 = (bf16[4,288,1024]{2,1,0:T(8,128)(2,1)S(1)}, bf16[4096,512]{1,0:T(8,128)(2,1)S(1)}) custom-call(s32[3]{0:T(128)S(1)} %pad_add_fusion.at_ref, bf16[16,288,128]{2,1,0:T(8,128)(2,1)S(1)} %bitcast.17, f32[1,2048]{1,0:T(1,128)S(1)} %bitcast.26, bf16[12288,128]{1,0:T(8,128)(2,1)} %get-tuple-element.25.own, bf16[12288,128]{1,0:T(8,128)(2,1)} %copy-done.7, ...), custom_call_target="tpu_custom_call" | custom-call | tf_op jit(solution)/shard_map/up/pallas_call | solution.py:450
  140.1 19.3 %all_to_all.45.act_ref = bf16[4,288,1024]{2,1,0:T(8,128)(2,1)S(1)} all-to-all(bf16[4,288,1024]{2,1,0:T(8,128)(2,1)S(1)} %get-tuple-element.32), channel_id=1, replica_groups={{0,4,8,12},{1,5,9,13},{2,6,10,14},{3,7,11,15},{16,17,18,19},{20,21,22,2..., dimensions={0} | all-to-all | bytes 4718592 | tf_op jit(solution)/shard_map/all_to_all | solution.py:42
  159.3 0.0 copy-start.4
  159.3 1.9 shard_map.159
  161.3 8.1 %all_to_all.46 = bf16[4,288,128]{2,1,0:T(8,128)(2,1)S(1)} all-to-all(bf16[4,288,128]{2,1,0:T(8,128)(2,1)S(1)} %shard_map.159), channel_id=1, replica_groups={{0,1,2,3},{4,5,6,7},{8,9,10,11},{12,13,14,15},{16,20,24,28},{17,21,25,2..., dimensions={0} | all-to-all | bytes 589824 | tf_op jit(solution)/shard_map/all_to_all | solution.py:42
  169.4 19.0 %all_to_all.47 = bf16[16,72,128]{2,1,0:T(8,128)(2,1)S(1)} all-to-all(bf16[16,72,128]{2,1,0:T(8,128)(2,1)S(1)} %bitcast.29), channel_id=1, replica_groups=mesh['z'=16,'c'=2,'y'=4,'x'=4] {'z'}, dimensions={0} | all-to-all | bytes 589824 | tf_op jit(solution)/shard_map/all_to_all | solution.py:475
  188.3 10.0 %all-gather.3 = bf16[32,72,128]{2,1,0:T(8,128)(2,1)S(1)} all-gather(bf16[16,72,128]{2,1,0:T(8,128)(2,1)S(1)} %all_to_all.47), channel_id=5, replica_groups=mesh['z'=16,'c'=2,'y'=4,'x'=4] {'c'}, dimensions={0}, use_global_device_ids=true | all-gather | bytes 884736 | tf_op jit(solution)/shard_map/all_gather | solution.py:476
  198.3 0.0 copy-done.4
  198.4 2.8 %shard_map.160 = bf16[192,128]{1,0:T(8,128)(2,1)} custom-call(s32[3]{0:T(128)S(1)} %pad_add_fusion.at_ref, bf16[2,16,72,128]{3,2,1,0:T(8,128)(2,1)S(1)} %bitcast.20, bf16[192,128]{1,0:T(8,128)(2,1)S(1)} %get-tuple-element.34.stream_ref, s32[4,192]{1,0:T(4,128)S(1)} %bitcast.25, f32[4,192]{1,0:T(4,128)S(1)} %bitcast.27), custom_call_target="tpu_custom_call" | custom-call | tf_op jit(solution)/shard_map/pallas_call | solution.py:477
Async XLA Ops:
  0.1 52.0 %copy-start = (bf16[128,2048]{1,0:T(8,128)(2,1)S(1)}, bf16[128,2048]{1,0:T(8,128)(2,1)}, u32[]{:S(2)}) copy-start(bf16[128,2048]{1,0:T(8,128)(2,1)} %w_ref.1) | copy-start | bytes 1572868
  0.1 52.0 %copy-start.1 = (bf16[192,128]{1,0:T(8,128)(2,1)S(1)}, bf16[192,128]{1,0:T(8,128)(2,1)}, u32[]{:S(2)}) copy-start(bf16[192,128]{1,0:T(8,128)(2,1)} %gate_ref.1) | copy-start | bytes 147460
  0.1 52.0 %copy-start.5 = (f32[128]{0:T(128)S(1)}, f32[128]{0:T(128)}, u32[]{:S(2)}) copy-start(f32[128]{0:T(128)} %param.24) | copy-start | bytes 1540
  4.2 70.9 %collective-permute-start.1 = (bf16[12288,128]{1,0:T(8,128)(2,1)}, bf16[12288,128]{1,0:T(8,128)(2,1)S(1)}, u32[]{:S(2)}, u32[]{:S(2)}) collective-permute-start(bf16[12288,128]{1,0:T(8,128)(2,1)} %get-tuple-element.25.own), channel_id=1, source_target_pairs={{0,3},{1,0},{2,1},{3,2},{4,7},{5,4},{6,5},{7,6},{8,11},{9,8},{10,9... | collective-permute-start | bytes 9437192 | tf_op jit(solution)/shard_map/ppermute | solution.py:55
  9.7 65.5 %collective-permute-start = (bf16[12288,128]{1,0:T(8,128)(2,1)}, bf16[12288,128]{1,0:T(8,128)(2,1)S(1)}, u32[]{:S(2)}, u32[]{:S(2)}) collective-permute-start(bf16[12288,128]{1,0:T(8,128)(2,1)} %get-tuple-element.25.own), channel_id=1, source_target_pairs={{0,1},{1,2},{2,3},{3,0},{4,5},{5,6},{6,7},{7,4},{8,9},{9,10},{10,1... | collective-permute-start | bytes 9437192 | tf_op jit(solution)/shard_map/ppermute | solution.py:55
  19.1 54.9 %copy-start.2 = (s32[192,4]{0,1:T(4,128)S(1)}, s32[192,4]{0,1:T(4,128)}, u32[]{:S(2)}) copy-start(s32[192,4]{0,1:T(4,128)} %param.27) | copy-start | bytes 9220
  75.1 1.7 copy-start.6
  75.2 2.8 %copy-start.7 = (bf16[12288,128]{1,0:T(8,128)(2,1)}, bf16[12288,128]{1,0:T(8,128)(2,1)S(1)}, u32[]{:S(2)}) copy-start(bf16[12288,128]{1,0:T(8,128)(2,1)S(1)} %collective-permute-done.plus) | copy-start | bytes 9437188
  77.9 42.7 %collective-permute-start.3 = (bf16[6144,128]{1,0:T(8,128)(2,1)S(1)}, bf16[6144,128]{1,0:T(8,128)(2,1)S(1)}, u32[]{:S(2)}, u32[]{:S(2)}) collective-permute-start(bf16[6144,128]{1,0:T(8,128)(2,1)S(1)} %slice.7), channel_id=1, source_target_pairs={{0,3},{1,0},{2,1},{3,2},{4,7},{5,4},{6,5},{7,6},{8,11},{9,8},{10,9... | collective-permute-start | bytes 4718600 | tf_op jit(solution)/shard_map/ppermute | solution.py:55
  80.4 40.2 %collective-permute-start.2 = (bf16[6144,128]{1,0:T(8,128)(2,1)S(1)}, bf16[6144,128]{1,0:T(8,128)(2,1)S(1)}, u32[]{:S(2)}, u32[]{:S(2)}) collective-permute-start(bf16[6144,128]{1,0:T(8,128)(2,1)S(1)} %slice.6), channel_id=1, source_target_pairs={{0,1},{1,2},{2,3},{3,0},{4,5},{5,6},{6,7},{7,4},{8,9},{9,10},{10,1... | collective-permute-start | bytes 4718600 | tf_op jit(solution)/shard_map/ppermute | solution.py:55
  112.3 21.7 %copy-start.3 = (f32[2048]{0:T(1024)S(1)}, f32[2048]{0:T(1024)}, u32[]{:S(2)}) copy-start(f32[2048]{0:T(1024)} %param.26) | copy-start | bytes 24580
  120.6 13.3 %copy-start.8 = (bf16[6144,128]{1,0:T(8,128)(2,1)}, bf16[6144,128]{1,0:T(8,128)(2,1)S(1)}, u32[]{:S(2)}) copy-start(bf16[6144,128]{1,0:T(8,128)(2,1)S(1)} %collective-permute-done.3.far1) | copy-start | bytes 4718596
  120.6 13.3 %copy-start.9 = (bf16[6144,128]{1,0:T(8,128)(2,1)}, bf16[6144,128]{1,0:T(8,128)(2,1)S(1)}, u32[]{:S(2)}) copy-start(bf16[6144,128]{1,0:T(8,128)(2,1)S(1)} %collective-permute-done.2.far0) | copy-start | bytes 4718596
  159.3 39.0 %copy-start.4 = (f32[192,4]{0,1:T(4,128)S(1)}, f32[192,4]{0,1:T(4,128)}, u32[]{:S(2)}) copy-start(f32[192,4]{0,1:T(4,128)} %param.28) | copy-start | bytes 9220

commit v4 on v3

--- a/solution.py
+++ b/solution.py
@@ -15,7 +15,6 @@
 R = 192
 W = 128
 D = 2048
-SLOTS = 1152
 PART = 288
 SIDE = 4
 TP = SIDE * SIDE
@@ -119,18 +118,15 @@
     inward = []
     outward = []
     for k, w_hbm in enumerate((wg_hbm, wg_hbm, wu_hbm, wu_hbm, wd_hbm)):
+        rows = pl.ds(k * D, 2 * D if k == 4 else D)
         source = w_hbm if k == 4 else w_hbm.at[:, pl.ds((k % 2) * W, W)]
-        held = held_ref.at[pl.ds(k * D, 2 * D if k == 4 else D)]
-        target = joined_hbm.at[pl.ds(k * D, 2 * D if k == 4 else D)]
+        held = held_ref.at[rows]
         inward.append(pltpu.make_async_copy(source, held, sems.at[7 + k]))
-        outward.append(pltpu.make_async_copy(held, target, sems.at[12 + k]))
+        outward.append(pltpu.make_async_copy(held, joined_hbm.at[rows], sems.at[12 + k]))
     for copy in copies + inward:
         copy.start()
     for copy in copies:
         copy.wait()
-    for first, second in zip(inward, outward):
-        first.wait()
-        second.start()
     q = q_ref[...].astype(F32)
     q = q * jax.nn.sigmoid(q)
     v = v_ref[...]
@@ -140,6 +136,10 @@
     jc = jnp.sum(jnp.where(row == col, jr, 0.0), axis=1, keepdims=True)
     total = None
     for d, f_ref in enumerate((ff_ref, fb_ref)):
+        if d == 1:
+            for first, second in zip(inward, outward):
+                first.wait()
+                second.start()
         seen = (col <= row) if d == 0 else (col >= row)
         seen_t = (row <= col) if d == 0 else (row >= col)
         key = gap_ref[d : d + 1, :] * jax.nn.sigmoid(-f_ref[...].astype(F32))
@@ -250,16 +250,22 @@
     choose = (source == wanted).astype(BF16)
     for z in range(Z):
         both = jnp.concatenate([got_ref[0, z], got_ref[1, z]], axis=0)
-        out_ref[z * PAIR : (z + 1) * PAIR, :] = dot(choose, both, ((1,), (0,))).astype(BF16)
+        rows = dot(choose, both, ((1,), (0,))).astype(BF16)
+        a, place_in = divmod(z, SIDE)
+        for b in range(SIDE):
+            target = jnp.where(c == 0, b * SIDE + a, a * SIDE + b)
+            out_ref[target, place_in * PAIR : (place_in + 1) * PAIR, :] = rows
 
 
 def up_body(
-    at_ref, x_ref, gain_ref, own, plus, minus, far0, far1, out_ref, wd_ref, w_ref, rows_ref, sems
+    x_ref, gain_ref, wg, wu, wd, plus, minus, far0, far1, out_ref, wd_ref, w_ref, rows_ref, sems
 ):
     def piece(q, k, rows):
         start = k * D
+        if q == 0:
+            return wd if k == 4 else (wg, wu)[k // 2].at[:, pl.ds((k % 2) * W, W)]
         if q < 3:
-            return (own, plus, minus)[q].at[pl.ds(start, rows)]
+            return (plus, minus)[q - 1].at[pl.ds(start, rows)]
         return (far0, far1)[start // (3 * D)].at[pl.ds(start % (3 * D), rows)]
 
     copies = []
@@ -272,15 +278,13 @@
         copies.append(pltpu.make_async_copy(piece(q, 4, 2 * D), target, sems.at[5 * q + 4]))
     for copy in copies:
         copy.start()
-    turned = at_ref[1] == 1
     squares = None
     for p in range(TP):
         x = x_ref[p].astype(F32)
         squares = x * x if squares is None else squares + x * x
     scale = lax.rsqrt(jnp.sum(squares, axis=1, keepdims=True) / D + EPS)
     for p in range(TP):
-        share = jnp.where(turned, (p % SIDE) * SIDE + p // SIDE, p)
-        cols = pl.ds(pl.multiple_of(share * W, W), W)
+        cols = pl.ds(p * W, W)
         rows_ref[:, cols] = (x_ref[p].astype(F32) * scale * gain_ref[:, cols]).astype(BF16)
     rows = rows_ref[...]
     for q in range(SIDE):
@@ -314,7 +318,24 @@
         out_ref[along(at_ref, q)] = made[:, q * W : (q + 1) * W]
 
 
-def return_body(at_ref, got_ref, stream_ref, ids_ref, weights_ref, out_ref):
+def halves_body(plus_hbm, minus_hbm, first_hbm, second_hbm, held_ref, sems):
+    half = 3 * D
+    parts = ((plus_hbm.at[pl.ds(0, half)], first_hbm), (minus_hbm.at[pl.ds(half, half)], second_hbm))
+    inward = []
+    outward = []
+    for k, (source, target) in enumerate(parts):
+        inward.append(pltpu.make_async_copy(source, held_ref.at[k], sems.at[k]))
+        outward.append(pltpu.make_async_copy(held_ref.at[k], target, sems.at[2 + k]))
+    for copy in inward:
+        copy.start()
+    for first, second in zip(inward, outward):
+        first.wait()
+        second.start()
+    for copy in outward:
+        copy.wait()
+
+
+def shares_body(at_ref, ids_ref, weights_ref, high_ref, low_ref):
     ids = ids_ref[...]
     weights = weights_ref[...]
     group = iota2((32, R), 0)
@@ -331,10 +352,14 @@
     rank = (place_in - at_ref[1] * CAP).astype(F32)
     high, low = split(share)
     slot_at = dot(slots.astype(BF16), spread, ((0,), (0,)))
-    share_at = dot(high, spread, ((0,), (0,))) + dot(low, spread, ((0,), (0,)))
-    mixing = jnp.where(slot_at == rank, share_at, 0.0)
+    hit = slot_at == rank
+    high_ref[...] = jnp.where(hit, dot(high, spread, ((0,), (0,))), 0.0).astype(BF16)
+    low_ref[...] = jnp.where(hit, dot(low, spread, ((0,), (0,))), 0.0).astype(BF16)
+
+
+def return_body(got_ref, stream_ref, high_ref, low_ref, out_ref):
     got = jnp.concatenate([got_ref[k, z] for k in range(2) for z in range(Z)], axis=0)
-    total = dot2(mixing, got, ((1,), (0,)))
+    total = dot(high_ref[...], got, ((1,), (0,))) + dot(low_ref[...], got, ((1,), (0,)))
     out_ref[...] = (stream_ref[...].astype(F32) + total).astype(BF16)
 
 
@@ -352,13 +377,13 @@
     return pltpu.with_memory_space_constraint(x, pltpu.HBM)
 
 
-def whole(body, outs, specs):
+def whole(body, outs, specs, room=12):
     return pl.pallas_call(
         body,
         out_shape=[jax.ShapeDtypeStruct(s, t) for s, t in outs],
         in_specs=specs,
         out_specs=[VMEM] * len(outs),
-        compiler_params=limit(12),
+        compiler_params=limit(room),
     )
 
 
@@ -438,14 +463,29 @@
     )(at, terms, own_residual, ids)
 
     buffer, plus, minus = lax.optimization_barrier((buffer, plus, minus))
-    far0 = passed_on(plus[: 3 * D], 1)
-    far1 = passed_on(minus[3 * D :], SIDE - 1)
+    first_half, second_half = pl.pallas_call(
+        halves_body,
+        out_shape=[pltpu.HBM((3 * D, W), BF16)] * 2,
+        in_specs=[HBM, HBM],
+        out_specs=[HBM, HBM],
+        scratch_shapes=[pltpu.VMEM((2, 3 * D, W), BF16), pltpu.SemaphoreType.DMA((4,))],
+        compiler_params=limit(8),
+        name="halves",
+    )(in_hbm(plus), in_hbm(minus))
+    far0 = passed_on(first_half, 1)
+    far1 = passed_on(second_half, SIDE - 1)
     arrived = lax.all_to_all(buffer, "z", 0, 0, tiled=True)
+    high, low = pl.pallas_call(
+        shares_body,
+        out_shape=[pltpu.VMEM((R, 32 * PAIR), BF16)] * 2,
+        in_specs=[SMEM, VMEM, VMEM],
+        out_specs=[IN_VMEM, IN_VMEM],
+        compiler_params=limit(12),
+        name="shares",
+    )(at, ids, weights)
     arrived = lax.all_gather(arrived, "c")
-    (rows,) = whole(pick_body, (((SLOTS, W), BF16),), [SMEM, VMEM])(at, arrived)
-    rows = exchange(rows.reshape(SIDE, PART, W), FIRST)
-    rows, far0, far1 = lax.optimization_barrier((rows, far0, far1))
-    rows = exchange(jnp.broadcast_to(rows, (SIDE, *rows.shape)), SECOND).reshape(TP, PART, W)
+    (rows,) = whole(pick_body, (((TP, PART, W), BF16),), [SMEM, VMEM])(at, arrived)
+    rows = lax.all_to_all(rows, PLANE, 0, 0, tiled=True)
 
     active, down = pl.pallas_call(
         up_body,
@@ -453,7 +493,7 @@
             jax.ShapeDtypeStruct((SIDE, PART, SIDE * HID), BF16),
             pltpu.VMEM((2 * D, SIDE * W), BF16),
         ],
-        in_specs=[SMEM, VMEM, VMEM] + [HBM] * 5,
+        in_specs=[VMEM, VMEM] + [HBM] * 7,
         out_specs=[VMEM, IN_VMEM],
         scratch_shapes=[
             pltpu.VMEM((SIDE, 2, D, HID), BF16),
@@ -463,10 +503,9 @@
         compiler_params=limit(24),
         name="up",
     )(
-        at,
         rows,
         norm_gain.reshape(1, D),
-        *(in_hbm(w) for w in (joined, plus, minus, far0, far1)),
+        *(in_hbm(w) for w in (w_gate[0], w_up[0], w_down[0], plus, minus, far0, far1)),
     )
     active = exchange(active, SECOND)
     (made,) = whole(down_body, (((SIDE, PART, W), BF16),), [SMEM, VMEM, VMEM])(at, active, down)
@@ -474,8 +513,8 @@
 
     back = lax.all_to_all(produced.reshape(Z, PAIR, W), "z", 0, 0, tiled=True)
     back = lax.all_gather(back, "c")
-    (mixed,) = whole(return_body, (((R, W), BF16),), [SMEM] + [VMEM] * 4)(
-        at, back, stream, ids, weights
+    (mixed,) = whole(return_body, (((R, W), BF16),), [VMEM, VMEM, IN_VMEM, IN_VMEM])(
+        back, stream, high, low
     )
     return mixed
 

time: 202 us -> 194 us (0.960)
  the two profiles are of different devices: /device:TPU:1 before, /device:TPU:33 now
where the time goes in v4:
time: 194 us; the launch traced here: 193 us
  blocking collectives  100 us (52%)
  waiting for transfers between devices  41.3 us (21%)
  starting transfers between devices  28.2 us (15%)
  Pallas kernels  23.3 us (12%)
    all_to_all x1, blocking collectives, shards(): packed = lax.all_to_all(packed, 'z', 0, 0, tiled=True)  33.2 us
    all_to_all x2, blocking collectives, exchange(): lax.all_to_all(pieces, CYX, 0, 0, axis_index_groups=groups, tiled=True)  28.3 us
    all_to_all x1, blocking collectives, shards(): terms = lax.all_to_all(terms, PLANE, 0, 0, tiled=True)  19.2 us
    all_to_all x1, waiting for transfers between devices, shards(): rows = lax.all_to_all(rows, PLANE, 0, 0, tiled=True)  19.1 us
    all_to_all x1, waiting for transfers between devices, shards(): back = lax.all_to_all(produced.reshape(Z, PAIR, W), 'z', 0, 0, tiled=True)  13.1 us
    ppermute x4, starting transfers between devices, passed_on(): return lax.ppermute(x, CYX, ring(step))  13.1 us
    all_gather x1, blocking collectives, shards(): back = lax.all_gather(back, 'c')  10.3 us
    all_to_all x1, waiting for transfers between devices, shards(): arrived = lax.all_to_all(buffer, 'z', 0, 0, tiled=True)  9.04 us
  transfers between devices with their start and end apart: 7, of which 3 were waited for; matrix products, arithmetic and copies ran while one was open for 0% of the time, Pallas kernels for 6%

profile of v4, /device:TPU:33, one launch (start us, length us, event | category | flops | bytes accessed | tf_op | source)
XLA Modules:
  0.0 193.4 jit_solution(16356918368798059254)
XLA Ops:
  0.0 0.1 pad_add_fusion.at_ref
  0.1 0.0 copy-start
  0.1 0.0 copy-start.1
  0.1 0.0 copy-start.5
  0.1 4.0 %head.1 = (f32[192,128]{1,0:T(8,128)S(1)}, f32[2,192,128]{2,1,0:T(8,128)S(1)}, f32[2,136,128]{2,1,0:T(8,128)S(1)}, bf16[192,128]{1,0:T(8,128)(2,1)S(1)}, bf16[12288,128]{1,0:T(8,128)(2,1)}) custom-call(s32[3]{0:T(128)S(1)} %pad_add_fusion.at_ref, bf16[192,128]{1,0:T(8,128)(2,1)} %q_hbm.1, bf16[192,128]{1,0:T(8,128)(2,1)} %v_hbm.1, bf16[192,128]{1,0:T(8,128)(2,1)} %ff_hbm.1, ...), custom_call_target="tpu_custom_call" | custom-call | tf_op jit(solution)/shard_map/head/pallas_call | solution.py:415
  4.1 3.2 %collective-permute-start = (bf16[12288,128]{1,0:T(8,128)(2,1)}, bf16[12288,128]{1,0:T(8,128)(2,1)}, u32[]{:S(2)}, u32[]{:S(2)}) collective-permute-start(bf16[12288,128]{1,0:T(8,128)(2,1)} %get-tuple-element.26), channel_id=1, source_target_pairs={{0,1},{1,2},{2,3},{3,0},{4,5},{5,6},{6,7},{7,4},{8,9},{9,10},{10,1... | collective-permute-start | bytes 9437192 | tf_op jit(solution)/shard_map/ppermute | solution.py:54
  7.3 3.4 %collective-permute-start.1 = (bf16[12288,128]{1,0:T(8,128)(2,1)}, bf16[12288,128]{1,0:T(8,128)(2,1)}, u32[]{:S(2)}, u32[]{:S(2)}) collective-permute-start(bf16[12288,128]{1,0:T(8,128)(2,1)} %get-tuple-element.26), channel_id=1, source_target_pairs={{0,3},{1,0},{2,1},{3,2},{4,7},{5,4},{6,5},{7,6},{8,11},{9,8},{10,9... | collective-permute-start | bytes 9437192 | tf_op jit(solution)/shard_map/ppermute | solution.py:54
  10.6 2.8 %all-gather = f32[4,136,128]{2,1,0:T(8,128)S(1)} all-gather(f32[2,136,128]{2,1,0:T(8,128)S(1)} %get-tuple-element.23), channel_id=2, replica_groups=mesh['z'=16,'c'=2,'y'=4,'x'=4] {'c'}, dimensions={0}, use_global_device_ids=true | all-gather | bytes 417792 | tf_op jit(solution)/shard_map/all_gather | solution.py:451
  13.4 0.6 shard_map.154
  14.0 0.0 copy-start.2
  14.1 33.2 %all_to_all.35.got_ref = bf16[16,72,128]{2,1,0:T(8,128)(2,1)S(1)} all-to-all(bf16[16,72,128]{2,1,0:T(8,128)(2,1)S(1)} %shard_map.154), channel_id=1, replica_groups=mesh['z'=16,'c'=2,'y'=4,'x'=4] {'z'}, dimensions={0} | all-to-all | bytes 589824 | tf_op jit(solution)/shard_map/all_to_all | solution.py:453
  47.3 0.7 shard_map.155
  48.0 3.2 %all-gather.1 = f32[4,64,128]{2,1,0:T(8,128)S(1)} all-gather(f32[2,64,128]{2,1,0:T(8,128)S(1)} %shard_map.155), channel_id=3, replica_groups=mesh['z'=16,'c'=2,'y'=4,'x'=4] {'c'}, dimensions={0}, use_global_device_ids=true | all-gather | bytes 196608 | tf_op jit(solution)/shard_map/all_gather | solution.py:455
  51.2 0.0 copy-done
  51.2 0.0 copy-done.1
  51.2 0.0 copy-done.5
  51.2 1.4 shard_map.156
  52.6 19.2 %all_to_all.36.got_ref = bf16[16,192,128]{2,1,0:T(8,128)(2,1)S(1)} all-to-all(bf16[16,192,128]{2,1,0:T(8,128)(2,1)S(1)} %shard_map.156), channel_id=1, replica_groups=mesh['z'=16,'c'=2,'y'=4,'x'=4] {'y','x'}, dimensions={0} | all-to-all | bytes 1572864 | tf_op jit(solution)/shard_map/all_to_all | solution.py:459
  71.8 0.0 copy-done.2
  71.8 1.8 shard_map.157
  73.5 0.0 collective-permute-done.plus_hbm.plus
  73.5 0.0 collective-permute-done.1.minus_hbm.minus
  73.5 5.8 %all-to-all-start.2 = ((bf16[16,72,128]{2,1,0:T(8,128)(2,1)}), bf16[16,72,128]{2,1,0:T(8,128)(2,1)S(1)}, u32[]{:S(2)}, u32[]{:S(2)}) async-start(bf16[16,72,128]{2,1,0:T(8,128)(2,1)} %get-tuple-element.27), calls=%async_computation.2 | async-start | bytes 589824 | tf_op jit(solution)/shard_map/all_to_all | solution.py:477
  79.4 3.2 %halves.1 = (bf16[6144,128]{1,0:T(8,128)(2,1)}, bf16[6144,128]{1,0:T(8,128)(2,1)}) custom-call(bf16[12288,128]{1,0:T(8,128)(2,1)} %collective-permute-done.plus_hbm.plus, bf16[12288,128]{1,0:T(8,128)(2,1)} %collective-permute-done.1.minus_hbm.minus), custom_call_target="tpu_custom_call" | custom-call | tf_op jit(solution)/shard_map/halves/pallas_call | solution.py:466
  82.6 1.9 collective-permute-start.2
  84.5 0.0 copy-start.3
  84.5 4.6 %collective-permute-start.3 = (bf16[6144,128]{1,0:T(8,128)(2,1)}, bf16[6144,128]{1,0:T(8,128)(2,1)}, u32[]{:S(2)}, u32[]{:S(2)}) collective-permute-start(bf16[6144,128]{1,0:T(8,128)(2,1)} %get-tuple-element.31), channel_id=1, source_target_pairs={{0,3},{1,0},{2,1},{3,2},{4,7},{5,4},{6,5},{7,6},{8,11},{9,8},{10,9... | collective-permute-start | bytes 4718600 | tf_op jit(solution)/shard_map/ppermute | solution.py:54
  89.1 9.0 %all-to-all-done.2 = bf16[16,72,128]{2,1,0:T(8,128)(2,1)S(1)} async-done(((bf16[16,72,128]{2,1,0:T(8,128)(2,1)}), bf16[16,72,128]{2,1,0:T(8,128)(2,1)S(1)}, u32[]{:S(2)}, u32[]{:S(2)}) %all-to-all-start.2) | async-done | bytes 294944 | tf_op jit(solution)/shard_map/all_to_all | solution.py:477
  98.1 3.4 %all-gather.2 = bf16[32,72,128]{2,1,0:T(8,128)(2,1)S(1)} all-gather(bf16[16,72,128]{2,1,0:T(8,128)(2,1)S(1)} %all-to-all-done.2), channel_id=4, replica_groups=mesh['z'=16,'c'=2,'y'=4,'x'=4] {'c'}, dimensions={0}, use_global_device_ids=true | all-gather | bytes 884736 | tf_op jit(solution)/shard_map/all_gather | solution.py:486
  101.5 1.9 shard_map.158
  103.4 3.7 %all-to-all-start.3 = ((bf16[16,288,128]{2,1,0:T(8,128)(2,1)}), bf16[16,288,128]{2,1,0:T(8,128)(2,1)S(1)}, u32[]{:S(2)}, u32[]{:S(2)}) async-start(bf16[16,288,128]{2,1,0:T(8,128)(2,1)} %shard_map.158), calls=%async_computation.3 | async-start | bytes 2359296 | tf_op jit(solution)/shard_map/all_to_all | solution.py:488
  107.1 0.0 collective-permute-done.2.far0
  107.2 0.0 copy-start.6
  107.2 0.0 collective-permute-done.3.far1
  107.2 19.1 %all-to-all-done.3.x_ref = bf16[16,288,128]{2,1,0:T(8,128)(2,1)S(1)} async-done(((bf16[16,288,128]{2,1,0:T(8,128)(2,1)}), bf16[16,288,128]{2,1,0:T(8,128)(2,1)S(1)}, u32[]{:S(2)}, u32[]{:S(2)}) %all-to-all-start.3) | async-done | bytes 1179680 | tf_op jit(solution)/shard_map/all_to_all | solution.py:488
  126.3 0.0 copy-done.6
  126.3 0.0 copy-done.3
  126.3 4.9 %up.1 = (bf16[4,288,1024]{2,1,0:T(8,128)(2,1)S(1)}, bf16[4096,512]{1,0:T(8,128)(2,1)S(1)}) custom-call(bf16[16,288,128]{2,1,0:T(8,128)(2,1)S(1)} %all-to-all-done.3.x_ref, f32[1,2048]{1,0:T(1,128)S(1)} %bitcast.22, bf16[2048,256]{1,0:T(8,128)(2,1)} %bitcast.26, bf16[2048,256]{1,0:T(8,128)(2,1)} %bitcast.28, bf16[4096,128]{1,0:T(8,128)(2,1)} %bitcast.30, ...), custom_call_target="tpu_custom_call" | custom-call | tf_op jit(solution)/shard_map/up/pallas_call | solution.py:490
  131.2 19.5 %all_to_all.37.act_ref = bf16[4,288,1024]{2,1,0:T(8,128)(2,1)S(1)} all-to-all(bf16[4,288,1024]{2,1,0:T(8,128)(2,1)S(1)} %get-tuple-element.32), channel_id=1, replica_groups={{0,4,8,12},{1,5,9,13},{2,6,10,14},{3,7,11,15},{16,17,18,19},{20,21,22,2..., dimensions={0} | all-to-all | bytes 4718592 | tf_op jit(solution)/shard_map/all_to_all | solution.py:41
  150.7 0.0 copy-start.4
  150.7 2.0 %shard_map.159 = bf16[4,288,128]{2,1,0:T(8,128)(2,1)S(1)} custom-call(s32[3]{0:T(128)S(1)} %pad_add_fusion.at_ref, bf16[4,288,1024]{2,1,0:T(8,128)(2,1)S(1)} %all_to_all.37.act_ref, bf16[4096,512]{1,0:T(8,128)(2,1)S(1)} %get-tuple-element.33.w_ref), custom_call_target="tpu_custom_call" | custom-call | tf_op jit(solution)/shard_map/pallas_call | solution.py:511
  152.7 8.8 %all_to_all.38 = bf16[4,288,128]{2,1,0:T(8,128)(2,1)} all-to-all(bf16[4,288,128]{2,1,0:T(8,128)(2,1)S(1)} %shard_map.159), channel_id=1, replica_groups={{0,1,2,3},{4,5,6,7},{8,9,10,11},{12,13,14,15},{16,20,24,28},{17,21,25,2..., dimensions={0} | all-to-all | bytes 589824 | tf_op jit(solution)/shard_map/all_to_all | solution.py:41
  161.5 5.7 %all-to-all-start.6 = ((bf16[16,72,128]{2,1,0:T(8,128)(2,1)}), bf16[16,72,128]{2,1,0:T(8,128)(2,1)S(1)}, u32[]{:S(2)}, u32[]{:S(2)}) async-start(bf16[16,72,128]{2,1,0:T(8,128)(2,1)} %bitcast.12), calls=%async_computation.6 | async-start | bytes 589824 | tf_op jit(solution)/shard_map/all_to_all | solution.py:514
  167.2 0.0 copy-done.4
  167.2 1.6 shares.1
  168.8 13.1 %all-to-all-done.6 = bf16[16,72,128]{2,1,0:T(8,128)(2,1)S(1)} async-done(((bf16[16,72,128]{2,1,0:T(8,128)(2,1)}), bf16[16,72,128]{2,1,0:T(8,128)(2,1)S(1)}, u32[]{:S(2)}, u32[]{:S(2)}) %all-to-all-start.6) | async-done | bytes 294944 | tf_op jit(solution)/shard_map/all_to_all | solution.py:514
  181.9 10.3 %all-gather.3 = bf16[32,72,128]{2,1,0:T(8,128)(2,1)S(1)} all-gather(bf16[16,72,128]{2,1,0:T(8,128)(2,1)S(1)} %all-to-all-done.6), channel_id=5, replica_groups=mesh['z'=16,'c'=2,'y'=4,'x'=4] {'c'}, dimensions={0}, use_global_device_ids=true | all-gather | bytes 884736 | tf_op jit(solution)/shard_map/all_gather | solution.py:515
  192.2 1.2 shard_map.160
Async XLA Ops:
  0.1 51.1 %copy-start = (bf16[128,2048]{1,0:T(8,128)(2,1)S(1)}, bf16[128,2048]{1,0:T(8,128)(2,1)}, u32[]{:S(2)}) copy-start(bf16[128,2048]{1,0:T(8,128)(2,1)} %w_ref.1) | copy-start | bytes 1572868
  0.1 51.1 %copy-start.1 = (bf16[192,128]{1,0:T(8,128)(2,1)S(1)}, bf16[192,128]{1,0:T(8,128)(2,1)}, u32[]{:S(2)}) copy-start(bf16[192,128]{1,0:T(8,128)(2,1)} %gate_ref.1) | copy-start | bytes 147460
  0.1 51.1 %copy-start.5 = (f32[128]{0:T(128)S(1)}, f32[128]{0:T(128)}, u32[]{:S(2)}) copy-start(f32[128]{0:T(128)} %param.24) | copy-start | bytes 1540
  4.1 69.5 %collective-permute-start = (bf16[12288,128]{1,0:T(8,128)(2,1)}, bf16[12288,128]{1,0:T(8,128)(2,1)}, u32[]{:S(2)}, u32[]{:S(2)}) collective-permute-start(bf16[12288,128]{1,0:T(8,128)(2,1)} %get-tuple-element.26), channel_id=1, source_target_pairs={{0,1},{1,2},{2,3},{3,0},{4,5},{5,6},{6,7},{7,4},{8,9},{9,10},{10,1... | collective-permute-start | bytes 9437192 | tf_op jit(solution)/shard_map/ppermute | solution.py:54
  7.3 66.3 %collective-permute-start.1 = (bf16[12288,128]{1,0:T(8,128)(2,1)}, bf16[12288,128]{1,0:T(8,128)(2,1)}, u32[]{:S(2)}, u32[]{:S(2)}) collective-permute-start(bf16[12288,128]{1,0:T(8,128)(2,1)} %get-tuple-element.26), channel_id=1, source_target_pairs={{0,3},{1,0},{2,1},{3,2},{4,7},{5,4},{6,5},{7,6},{8,11},{9,8},{10,9... | collective-permute-start | bytes 9437192 | tf_op jit(solution)/shard_map/ppermute | solution.py:54
  14.0 57.7 %copy-start.2 = (s32[192,4]{0,1:T(4,128)S(1)}, s32[192,4]{0,1:T(4,128)}, u32[]{:S(2)}) copy-start(s32[192,4]{0,1:T(4,128)} %param.27) | copy-start | bytes 9220
  73.5 24.6 %all-to-all-start.2 = ((bf16[16,72,128]{2,1,0:T(8,128)(2,1)}), bf16[16,72,128]{2,1,0:T(8,128)(2,1)S(1)}, u32[]{:S(2)}, u32[]{:S(2)}) async-start(bf16[16,72,128]{2,1,0:T(8,128)(2,1)} %get-tuple-element.27), calls=%async_computation.2 | async-start | bytes 589824 | tf_op jit(solution)/shard_map/all_to_all | solution.py:477
  82.6 24.6 %collective-permute-start.2 = (bf16[6144,128]{1,0:T(8,128)(2,1)}, bf16[6144,128]{1,0:T(8,128)(2,1)S(1)}, u32[]{:S(2)}, u32[]{:S(2)}) collective-permute-start(bf16[6144,128]{1,0:T(8,128)(2,1)} %get-tuple-element.30), channel_id=1, source_target_pairs={{0,1},{1,2},{2,3},{3,0},{4,5},{5,6},{6,7},{7,4},{8,9},{9,10},{10,1... | collective-permute-start | bytes 4718600 | tf_op jit(solution)/shard_map/ppermute | solution.py:54
  84.5 41.8 %copy-start.3 = (f32[2048]{0:T(1024)S(1)}, f32[2048]{0:T(1024)}, u32[]{:S(2)}) copy-start(f32[2048]{0:T(1024)} %param.26) | copy-start | bytes 24580
  84.5 22.6 %collective-permute-start.3 = (bf16[6144,128]{1,0:T(8,128)(2,1)}, bf16[6144,128]{1,0:T(8,128)(2,1)}, u32[]{:S(2)}, u32[]{:S(2)}) collective-permute-start(bf16[6144,128]{1,0:T(8,128)(2,1)} %get-tuple-element.31), channel_id=1, source_target_pairs={{0,3},{1,0},{2,1},{3,2},{4,7},{5,4},{6,5},{7,6},{8,11},{9,8},{10,9... | collective-permute-start | bytes 4718600 | tf_op jit(solution)/shard_map/ppermute | solution.py:54
  103.4 22.8 %all-to-all-start.3 = ((bf16[16,288,128]{2,1,0:T(8,128)(2,1)}), bf16[16,288,128]{2,1,0:T(8,128)(2,1)S(1)}, u32[]{:S(2)}, u32[]{:S(2)}) async-start(bf16[16,288,128]{2,1,0:T(8,128)(2,1)} %shard_map.158), calls=%async_computation.3 | async-start | bytes 2359296 | tf_op jit(solution)/shard_map/all_to_all | solution.py:488
  107.2 19.1 %copy-start.6 = (bf16[6144,128]{1,0:T(8,128)(2,1)}, bf16[6144,128]{1,0:T(8,128)(2,1)S(1)}, u32[]{:S(2)}) copy-start(bf16[6144,128]{1,0:T(8,128)(2,1)S(1)} %collective-permute-done.2.far0) | copy-start | bytes 4718596
  150.7 16.5 %copy-start.4 = (f32[192,4]{0,1:T(4,128)S(1)}, f32[192,4]{0,1:T(4,128)}, u32[]{:S(2)}) copy-start(f32[192,4]{0,1:T(4,128)} %param.28) | copy-start | bytes 9220
  161.5 20.4 %all-to-all-start.6 = ((bf16[16,72,128]{2,1,0:T(8,128)(2,1)}), bf16[16,72,128]{2,1,0:T(8,128)(2,1)S(1)}, u32[]{:S(2)}, u32[]{:S(2)}) async-start(bf16[16,72,128]{2,1,0:T(8,128)(2,1)} %bitcast.12), calls=%async_computation.6 | async-start | bytes 589824 | tf_op jit(solution)/shard_map/all_to_all | solution.py:514

commit v5 on v4

--- a/solution.py
+++ b/solution.py
@@ -229,7 +229,7 @@
     return jnp.where(named, rank, -1000.0)
 
 
-def send_body(at_ref, got_ref, res_ref, ids_ref, stream_ref, out_ref):
+def send_body(got_ref, res_ref, ids_ref, stream_ref, out_hbm, held_ref, sems):
     total = got_ref[0].astype(F32)
     for k in range(1, TP):
         total = total + got_ref[k].astype(F32)
@@ -237,24 +237,36 @@
     stream_ref[...] = stream
     slots = slots_of(ids_ref[...], iota2((32, R), 0))
     line = iota2((PAIR, R), 0).astype(F32)
+    copies = []
     for z in range(Z):
         hit = (line == slots[2 * z : 2 * z + 1]) | (line == slots[2 * z + 1 : 2 * z + 2] + CAP)
-        out_ref[z] = dot(hit.astype(BF16), stream, ((1,), (0,))).astype(BF16)
-
-
-def pick_body(at_ref, got_ref, out_ref):
+        held_ref[z] = dot(hit.astype(BF16), stream, ((1,), (0,))).astype(BF16)
+        copies.append(pltpu.make_async_copy(held_ref.at[z], out_hbm.at[z], sems.at[z]))
+        copies[z].start()
+    for copy in copies:
+        copy.wait()
+
+
+def pick_body(at_ref, got_ref, out_hbm, held_ref, sems):
     c = at_ref[1]
     line = iota2((PAIR, 2 * PAIR), 0)
     source = iota2((PAIR, 2 * PAIR), 1)
     wanted = line + c * CAP + jnp.where(line < CAP, 0, PAIR - CAP)
     choose = (source == wanted).astype(BF16)
-    for z in range(Z):
-        both = jnp.concatenate([got_ref[0, z], got_ref[1, z]], axis=0)
-        rows = dot(choose, both, ((1,), (0,))).astype(BF16)
-        a, place_in = divmod(z, SIDE)
+    copies = []
+    for a in range(SIDE):
+        for part in range(SIDE):
+            z = a * SIDE + part
+            both = jnp.concatenate([got_ref[0, z], got_ref[1, z]], axis=0)
+            rows = dot(choose, both, ((1,), (0,))).astype(BF16)
+            held_ref[a, part * PAIR : (part + 1) * PAIR, :] = rows
         for b in range(SIDE):
             target = jnp.where(c == 0, b * SIDE + a, a * SIDE + b)
-            out_ref[target, place_in * PAIR : (place_in + 1) * PAIR, :] = rows
+            k = a * SIDE + b
+            copies.append(pltpu.make_async_copy(held_ref.at[a], out_hbm.at[target], sems.at[k]))
+            copies[k].start()
+    for copy in copies:
+        copy.wait()
 
 
 def up_body(
@@ -458,9 +470,15 @@
     )
     terms = lax.all_to_all(terms, PLANE, 0, 0, tiled=True)
 
-    stream, buffer = whole(
-        send_body, (((R, W), BF16), ((Z, PAIR, W), BF16)), [SMEM] + [VMEM] * 3
-    )(at, terms, own_residual, ids)
+    stream, buffer = pl.pallas_call(
+        send_body,
+        out_shape=[jax.ShapeDtypeStruct((R, W), BF16), pltpu.HBM((Z, PAIR, W), BF16)],
+        in_specs=[VMEM] * 3,
+        out_specs=[VMEM, HBM],
+        scratch_shapes=[pltpu.VMEM((Z, PAIR, W), BF16), pltpu.SemaphoreType.DMA((Z,))],
+        compiler_params=limit(12),
+        name="send",
+    )(terms, own_residual, ids)
 
     buffer, plus, minus = lax.optimization_barrier((buffer, plus, minus))
     first_half, second_half = pl.pallas_call(
@@ -475,6 +493,17 @@
     far0 = passed_on(first_half, 1)
     far1 = passed_on(second_half, SIDE - 1)
     arrived = lax.all_to_all(buffer, "z", 0, 0, tiled=True)
+    arrived = lax.all_gather(arrived, "c")
+    rows = pl.pallas_call(
+        pick_body,
+        out_shape=pltpu.HBM((TP, PART, W), BF16),
+        in_specs=[SMEM, VMEM],
+        out_specs=HBM,
+        scratch_shapes=[pltpu.VMEM((SIDE, PART, W), BF16), pltpu.SemaphoreType.DMA((TP,))],
+        compiler_params=limit(12),
+        name="pick",
+    )(at, arrived)
+    rows = lax.all_to_all(rows, PLANE, 0, 0, tiled=True)
     high, low = pl.pallas_call(
         shares_body,
         out_shape=[pltpu.VMEM((R, 32 * PAIR), BF16)] * 2,
@@ -483,9 +512,6 @@
         compiler_params=limit(12),
         name="shares",
     )(at, ids, weights)
-    arrived = lax.all_gather(arrived, "c")
-    (rows,) = whole(pick_body, (((TP, PART, W), BF16),), [SMEM, VMEM])(at, arrived)
-    rows = lax.all_to_all(rows, PLANE, 0, 0, tiled=True)
 
     active, down = pl.pallas_call(
         up_body,

time: 194 us -> 194 us (level)
  transfers between devices with their start and end apart: 7 -> 7, of which waited for: 3 -> 3; matrix products, arithmetic and copies ran while one was open for 0% -> 0% of each run, Pallas kernels for 6% -> 5%
where the time goes in v5:
time: 194 us; the launch traced here: 193 us
  blocking collectives  100 us (52%)
  waiting for transfers between devices  41.3 us (21%)
  starting transfers between devices  28.2 us (15%)
  Pallas kernels  22.7 us (12%)
    all_to_all x1, blocking collectives, shards(): packed = lax.all_to_all(packed, 'z', 0, 0, tiled=True)  33.2 us
    all_to_all x2, blocking collectives, exchange(): lax.all_to_all(pieces, CYX, 0, 0, axis_index_groups=groups, tiled=True)  28.3 us
    all_to_all x1, blocking collectives, shards(): terms = lax.all_to_all(terms, PLANE, 0, 0, tiled=True)  19.2 us
    all_to_all x1, waiting for transfers between devices, shards(): rows = lax.all_to_all(rows, PLANE, 0, 0, tiled=True)  19.1 us
    all_to_all x1, waiting for transfers between devices, shards(): back = lax.all_to_all(produced.reshape(Z, PAIR, W), 'z', 0, 0, tiled=True)  13.1 us
    ppermute x4, starting transfers between devices, passed_on(): return lax.ppermute(x, CYX, ring(step))  13.1 us
    all_gather x1, blocking collectives, shards(): back = lax.all_gather(back, 'c')  10.3 us
    all_to_all x1, waiting for transfers between devices, shards(): arrived = lax.all_to_all(buffer, 'z', 0, 0, tiled=True)  9.04 us
  transfers between devices with their start and end apart: 7, of which 3 were waited for; matrix products, arithmetic and copies ran while one was open for 0% of the time, Pallas kernels for 5%

profile of v5, /device:TPU:33, one launch (start us, length us, event | category | flops | bytes accessed | tf_op | source)
XLA Modules:
  0.0 192.9 jit_solution(16675572704680350837)
XLA Ops:
  0.0 0.1 pad_add_fusion.at_ref
  0.1 0.0 copy-start
  0.1 0.0 copy-start.1
  0.1 0.0 copy-start.5
  0.1 4.0 %head.1 = (f32[192,128]{1,0:T(8,128)S(1)}, f32[2,192,128]{2,1,0:T(8,128)S(1)}, f32[2,136,128]{2,1,0:T(8,128)S(1)}, bf16[192,128]{1,0:T(8,128)(2,1)S(1)}, bf16[12288,128]{1,0:T(8,128)(2,1)}) custom-call(s32[3]{0:T(128)S(1)} %pad_add_fusion.at_ref, bf16[192,128]{1,0:T(8,128)(2,1)} %q_hbm.1, bf16[192,128]{1,0:T(8,128)(2,1)} %v_hbm.1, bf16[192,128]{1,0:T(8,128)(2,1)} %ff_hbm.1, ...), custom_call_target="tpu_custom_call" | custom-call | tf_op jit(solution)/shard_map/head/pallas_call | solution.py:427
  4.1 3.2 %collective-permute-start = (bf16[12288,128]{1,0:T(8,128)(2,1)}, bf16[12288,128]{1,0:T(8,128)(2,1)}, u32[]{:S(2)}, u32[]{:S(2)}) collective-permute-start(bf16[12288,128]{1,0:T(8,128)(2,1)} %get-tuple-element.26), channel_id=1, source_target_pairs={{0,1},{1,2},{2,3},{3,0},{4,5},{5,6},{6,7},{7,4},{8,9},{9,10},{10,1... | collective-permute-start | bytes 9437192 | tf_op jit(solution)/shard_map/ppermute | solution.py:54
  7.3 3.4 %collective-permute-start.1 = (bf16[12288,128]{1,0:T(8,128)(2,1)}, bf16[12288,128]{1,0:T(8,128)(2,1)}, u32[]{:S(2)}, u32[]{:S(2)}) collective-permute-start(bf16[12288,128]{1,0:T(8,128)(2,1)} %get-tuple-element.26), channel_id=1, source_target_pairs={{0,3},{1,0},{2,1},{3,2},{4,7},{5,4},{6,5},{7,6},{8,11},{9,8},{10,9... | collective-permute-start | bytes 9437192 | tf_op jit(solution)/shard_map/ppermute | solution.py:54
  10.6 2.8 %all-gather = f32[4,136,128]{2,1,0:T(8,128)S(1)} all-gather(f32[2,136,128]{2,1,0:T(8,128)S(1)} %get-tuple-element.23), channel_id=2, replica_groups=mesh['z'=16,'c'=2,'y'=4,'x'=4] {'c'}, dimensions={0}, use_global_device_ids=true | all-gather | bytes 417792 | tf_op jit(solution)/shard_map/all_gather | solution.py:463
  13.4 0.6 shard_map.154
  14.0 0.0 copy-start.2
  14.1 33.2 %all_to_all.35.got_ref = bf16[16,72,128]{2,1,0:T(8,128)(2,1)S(1)} all-to-all(bf16[16,72,128]{2,1,0:T(8,128)(2,1)S(1)} %shard_map.154), channel_id=1, replica_groups=mesh['z'=16,'c'=2,'y'=4,'x'=4] {'z'}, dimensions={0} | all-to-all | bytes 589824 | tf_op jit(solution)/shard_map/all_to_all | solution.py:465
  47.3 0.7 shard_map.155
  48.0 3.2 %all-gather.1 = f32[4,64,128]{2,1,0:T(8,128)S(1)} all-gather(f32[2,64,128]{2,1,0:T(8,128)S(1)} %shard_map.155), channel_id=3, replica_groups=mesh['z'=16,'c'=2,'y'=4,'x'=4] {'c'}, dimensions={0}, use_global_device_ids=true | all-gather | bytes 196608 | tf_op jit(solution)/shard_map/all_gather | solution.py:467
  51.2 0.0 copy-done
  51.2 0.0 copy-done.1
  51.2 0.0 copy-done.5
  51.2 1.4 shard_map.156
  52.6 19.2 %all_to_all.36.got_ref = bf16[16,192,128]{2,1,0:T(8,128)(2,1)S(1)} all-to-all(bf16[16,192,128]{2,1,0:T(8,128)(2,1)S(1)} %shard_map.156), channel_id=1, replica_groups=mesh['z'=16,'c'=2,'y'=4,'x'=4] {'y','x'}, dimensions={0} | all-to-all | bytes 1572864 | tf_op jit(solution)/shard_map/all_to_all | solution.py:471
  71.8 0.0 copy-done.2
  71.8 1.3 send.1
  73.0 0.0 collective-permute-done.plus_hbm.plus
  73.0 0.0 collective-permute-done.1.minus_hbm.minus
  73.0 5.8 %all-to-all-start.2 = ((bf16[16,72,128]{2,1,0:T(8,128)(2,1)}), bf16[16,72,128]{2,1,0:T(8,128)(2,1)S(1)}, u32[]{:S(2)}, u32[]{:S(2)}) async-start(bf16[16,72,128]{2,1,0:T(8,128)(2,1)} %get-tuple-element.27), calls=%async_computation.2 | async-start | bytes 589824 | tf_op jit(solution)/shard_map/all_to_all | solution.py:495
  78.9 3.2 %halves.1 = (bf16[6144,128]{1,0:T(8,128)(2,1)}, bf16[6144,128]{1,0:T(8,128)(2,1)}) custom-call(bf16[12288,128]{1,0:T(8,128)(2,1)} %collective-permute-done.plus_hbm.plus, bf16[12288,128]{1,0:T(8,128)(2,1)} %collective-permute-done.1.minus_hbm.minus), custom_call_target="tpu_custom_call" | custom-call | tf_op jit(solution)/shard_map/halves/pallas_call | solution.py:484
  82.1 1.9 collective-permute-start.2
  84.0 0.0 copy-start.3
  84.0 4.6 %collective-permute-start.3 = (bf16[6144,128]{1,0:T(8,128)(2,1)}, bf16[6144,128]{1,0:T(8,128)(2,1)}, u32[]{:S(2)}, u32[]{:S(2)}) collective-permute-start(bf16[6144,128]{1,0:T(8,128)(2,1)} %get-tuple-element.31), channel_id=1, source_target_pairs={{0,3},{1,0},{2,1},{3,2},{4,7},{5,4},{6,5},{7,6},{8,11},{9,8},{10,9... | collective-permute-start | bytes 4718600 | tf_op jit(solution)/shard_map/ppermute | solution.py:54
  88.6 9.0 %all-to-all-done.2 = bf16[16,72,128]{2,1,0:T(8,128)(2,1)S(1)} async-done(((bf16[16,72,128]{2,1,0:T(8,128)(2,1)}), bf16[16,72,128]{2,1,0:T(8,128)(2,1)S(1)}, u32[]{:S(2)}, u32[]{:S(2)}) %all-to-all-start.2) | async-done | bytes 294944 | tf_op jit(solution)/shard_map/all_to_all | solution.py:495
  97.7 3.4 %all-gather.2 = bf16[32,72,128]{2,1,0:T(8,128)(2,1)S(1)} all-gather(bf16[16,72,128]{2,1,0:T(8,128)(2,1)S(1)} %all-to-all-done.2), channel_id=4, replica_groups=mesh['z'=16,'c'=2,'y'=4,'x'=4] {'c'}, dimensions={0}, use_global_device_ids=true | all-gather | bytes 884736 | tf_op jit(solution)/shard_map/all_gather | solution.py:496
  101.1 1.9 pick.1
  103.0 3.7 %all-to-all-start.3 = ((bf16[16,288,128]{2,1,0:T(8,128)(2,1)}), bf16[16,288,128]{2,1,0:T(8,128)(2,1)S(1)}, u32[]{:S(2)}, u32[]{:S(2)}) async-start(bf16[16,288,128]{2,1,0:T(8,128)(2,1)} %pick.1), calls=%async_computation.3 | async-start | bytes 2359296 | tf_op jit(solution)/shard_map/all_to_all | solution.py:506
  106.7 0.0 collective-permute-done.2.far0
  106.7 0.0 copy-start.6
  106.7 0.0 collective-permute-done.3.far1
  106.7 19.1 %all-to-all-done.3.x_ref = bf16[16,288,128]{2,1,0:T(8,128)(2,1)S(1)} async-done(((bf16[16,288,128]{2,1,0:T(8,128)(2,1)}), bf16[16,288,128]{2,1,0:T(8,128)(2,1)S(1)}, u32[]{:S(2)}, u32[]{:S(2)}) %all-to-all-start.3) | async-done | bytes 1179680 | tf_op jit(solution)/shard_map/all_to_all | solution.py:506
  125.8 0.0 copy-done.6
  125.8 0.0 copy-done.3
  125.8 4.9 %up.1 = (bf16[4,288,1024]{2,1,0:T(8,128)(2,1)S(1)}, bf16[4096,512]{1,0:T(8,128)(2,1)S(1)}) custom-call(bf16[16,288,128]{2,1,0:T(8,128)(2,1)S(1)} %all-to-all-done.3.x_ref, f32[1,2048]{1,0:T(1,128)S(1)} %bitcast.22, bf16[2048,256]{1,0:T(8,128)(2,1)} %bitcast.26, bf16[2048,256]{1,0:T(8,128)(2,1)} %bitcast.28, bf16[4096,128]{1,0:T(8,128)(2,1)} %bitcast.30, ...), custom_call_target="tpu_custom_call" | custom-call | tf_op jit(solution)/shard_map/up/pallas_call | solution.py:516
  130.8 19.5 %all_to_all.37.act_ref = bf16[4,288,1024]{2,1,0:T(8,128)(2,1)S(1)} all-to-all(bf16[4,288,1024]{2,1,0:T(8,128)(2,1)S(1)} %get-tuple-element.32), channel_id=1, replica_groups={{0,4,8,12},{1,5,9,13},{2,6,10,14},{3,7,11,15},{16,17,18,19},{20,21,22,2..., dimensions={0} | all-to-all | bytes 4718592 | tf_op jit(solution)/shard_map/all_to_all | solution.py:41
  150.3 0.0 copy-start.4
  150.3 1.9 %shard_map.157 = bf16[4,288,128]{2,1,0:T(8,128)(2,1)S(1)} custom-call(s32[3]{0:T(128)S(1)} %pad_add_fusion.at_ref, bf16[4,288,1024]{2,1,0:T(8,128)(2,1)S(1)} %all_to_all.37.act_ref, bf16[4096,512]{1,0:T(8,128)(2,1)S(1)} %get-tuple-element.33.w_ref), custom_call_target="tpu_custom_call" | custom-call | tf_op jit(solution)/shard_map/pallas_call | solution.py:537
  152.2 8.8 %all_to_all.38 = bf16[4,288,128]{2,1,0:T(8,128)(2,1)} all-to-all(bf16[4,288,128]{2,1,0:T(8,128)(2,1)S(1)} %shard_map.157), channel_id=1, replica_groups={{0,1,2,3},{4,5,6,7},{8,9,10,11},{12,13,14,15},{16,20,24,28},{17,21,25,2..., dimensions={0} | all-to-all | bytes 589824 | tf_op jit(solution)/shard_map/all_to_all | solution.py:41
  161.0 5.6 %all-to-all-start.6 = ((bf16[16,72,128]{2,1,0:T(8,128)(2,1)}), bf16[16,72,128]{2,1,0:T(8,128)(2,1)S(1)}, u32[]{:S(2)}, u32[]{:S(2)}) async-start(bf16[16,72,128]{2,1,0:T(8,128)(2,1)} %bitcast.12), calls=%async_computation.6 | async-start | bytes 589824 | tf_op jit(solution)/shard_map/all_to_all | solution.py:540
  166.6 0.0 copy-done.4
  166.6 1.6 shares.1
  168.2 13.1 %all-to-all-done.6 = bf16[16,72,128]{2,1,0:T(8,128)(2,1)S(1)} async-done(((bf16[16,72,128]{2,1,0:T(8,128)(2,1)}), bf16[16,72,128]{2,1,0:T(8,128)(2,1)S(1)}, u32[]{:S(2)}, u32[]{:S(2)}) %all-to-all-start.6) | async-done | bytes 294944 | tf_op jit(solution)/shard_map/all_to_all | solution.py:540
  181.3 10.3 %all-gather.3 = bf16[32,72,128]{2,1,0:T(8,128)(2,1)S(1)} all-gather(bf16[16,72,128]{2,1,0:T(8,128)(2,1)S(1)} %all-to-all-done.6), channel_id=5, replica_groups=mesh['z'=16,'c'=2,'y'=4,'x'=4] {'c'}, dimensions={0}, use_global_device_ids=true | all-gather | bytes 884736 | tf_op jit(solution)/shard_map/all_gather | solution.py:541
  191.7 1.2 shard_map.158
Async XLA Ops:
  0.1 51.1 %copy-start = (bf16[128,2048]{1,0:T(8,128)(2,1)S(1)}, bf16[128,2048]{1,0:T(8,128)(2,1)}, u32[]{:S(2)}) copy-start(bf16[128,2048]{1,0:T(8,128)(2,1)} %w_ref.1) | copy-start | bytes 1572868
  0.1 51.1 %copy-start.1 = (bf16[192,128]{1,0:T(8,128)(2,1)S(1)}, bf16[192,128]{1,0:T(8,128)(2,1)}, u32[]{:S(2)}) copy-start(bf16[192,128]{1,0:T(8,128)(2,1)} %gate_ref.1) | copy-start | bytes 147460
  0.1 51.1 %copy-start.5 = (f32[128]{0:T(128)S(1)}, f32[128]{0:T(128)}, u32[]{:S(2)}) copy-start(f32[128]{0:T(128)} %param.24) | copy-start | bytes 1540
  4.1 69.0 %collective-permute-start = (bf16[12288,128]{1,0:T(8,128)(2,1)}, bf16[12288,128]{1,0:T(8,128)(2,1)}, u32[]{:S(2)}, u32[]{:S(2)}) collective-permute-start(bf16[12288,128]{1,0:T(8,128)(2,1)} %get-tuple-element.26), channel_id=1, source_target_pairs={{0,1},{1,2},{2,3},{3,0},{4,5},{5,6},{6,7},{7,4},{8,9},{9,10},{10,1... | collective-permute-start | bytes 9437192 | tf_op jit(solution)/shard_map/ppermute | solution.py:54
  7.3 65.8 %collective-permute-start.1 = (bf16[12288,128]{1,0:T(8,128)(2,1)}, bf16[12288,128]{1,0:T(8,128)(2,1)}, u32[]{:S(2)}, u32[]{:S(2)}) collective-permute-start(bf16[12288,128]{1,0:T(8,128)(2,1)} %get-tuple-element.26), channel_id=1, source_target_pairs={{0,3},{1,0},{2,1},{3,2},{4,7},{5,4},{6,5},{7,6},{8,11},{9,8},{10,9... | collective-permute-start | bytes 9437192 | tf_op jit(solution)/shard_map/ppermute | solution.py:54
  14.0 57.7 %copy-start.2 = (s32[192,4]{0,1:T(4,128)S(1)}, s32[192,4]{0,1:T(4,128)}, u32[]{:S(2)}) copy-start(s32[192,4]{0,1:T(4,128)} %param.27) | copy-start | bytes 9220
  73.0 24.6 %all-to-all-start.2 = ((bf16[16,72,128]{2,1,0:T(8,128)(2,1)}), bf16[16,72,128]{2,1,0:T(8,128)(2,1)S(1)}, u32[]{:S(2)}, u32[]{:S(2)}) async-start(bf16[16,72,128]{2,1,0:T(8,128)(2,1)} %get-tuple-element.27), calls=%async_computation.2 | async-start | bytes 589824 | tf_op jit(solution)/shard_map/all_to_all | solution.py:495
  82.1 24.6 %collective-permute-start.2 = (bf16[6144,128]{1,0:T(8,128)(2,1)}, bf16[6144,128]{1,0:T(8,128)(2,1)S(1)}, u32[]{:S(2)}, u32[]{:S(2)}) collective-permute-start(bf16[6144,128]{1,0:T(8,128)(2,1)} %get-tuple-element.30), channel_id=1, source_target_pairs={{0,1},{1,2},{2,3},{3,0},{4,5},{5,6},{6,7},{7,4},{8,9},{9,10},{10,1... | collective-permute-start | bytes 4718600 | tf_op jit(solution)/shard_map/ppermute | solution.py:54
  84.0 41.8 %copy-start.3 = (f32[2048]{0:T(1024)S(1)}, f32[2048]{0:T(1024)}, u32[]{:S(2)}) copy-start(f32[2048]{0:T(1024)} %param.26) | copy-start | bytes 24580
  84.0 22.7 %collective-permute-start.3 = (bf16[6144,128]{1,0:T(8,128)(2,1)}, bf16[6144,128]{1,0:T(8,128)(2,1)}, u32[]{:S(2)}, u32[]{:S(2)}) collective-permute-start(bf16[6144,128]{1,0:T(8,128)(2,1)} %get-tuple-element.31), channel_id=1, source_target_pairs={{0,3},{1,0},{2,1},{3,2},{4,7},{5,4},{6,5},{7,6},{8,11},{9,8},{10,9... | collective-permute-start | bytes 4718600 | tf_op jit(solution)/shard_map/ppermute | solution.py:54
  103.0 22.9 %all-to-all-start.3 = ((bf16[16,288,128]{2,1,0:T(8,128)(2,1)}), bf16[16,288,128]{2,1,0:T(8,128)(2,1)S(1)}, u32[]{:S(2)}, u32[]{:S(2)}) async-start(bf16[16,288,128]{2,1,0:T(8,128)(2,1)} %pick.1), calls=%async_computation.3 | async-start | bytes 2359296 | tf_op jit(solution)/shard_map/all_to_all | solution.py:506
  106.7 19.1 %copy-start.6 = (bf16[6144,128]{1,0:T(8,128)(2,1)}, bf16[6144,128]{1,0:T(8,128)(2,1)S(1)}, u32[]{:S(2)}) copy-start(bf16[6144,128]{1,0:T(8,128)(2,1)S(1)} %collective-permute-done.2.far0) | copy-start | bytes 4718596
  150.3 16.4 %copy-start.4 = (f32[192,4]{0,1:T(4,128)S(1)}, f32[192,4]{0,1:T(4,128)}, u32[]{:S(2)}) copy-start(f32[192,4]{0,1:T(4,128)} %param.28) | copy-start | bytes 9220
  161.0 20.3 %all-to-all-start.6 = ((bf16[16,72,128]{2,1,0:T(8,128)(2,1)}), bf16[16,72,128]{2,1,0:T(8,128)(2,1)S(1)}, u32[]{:S(2)}, u32[]{:S(2)}) async-start(bf16[16,72,128]{2,1,0:T(8,128)(2,1)} %bitcast.12), calls=%async_computation.6 | async-start | bytes 589824 | tf_op jit(solution)/shard_map/all_to_all | solution.py:540
